TPU v7x, 32 devices: a whole 2x2x4 slice. The times are simulated.
32 devices in a mesh: sp: 4 (over z), fs: 4 (over y, x), tp: 2 (over core).
Axes of the slice: x: 2, y: 2, z: 4, core: 2. Of those that a mesh axis runs over, the one named last changes fastest.
Arguments:
- tokens: bfloat16 [4, 3072, 2048], P('fs', 'sp', 'tp'), may hold values from -6 to 6
- in_gain: float32 [2048], replicated, may hold values from 0.1 to 1.9
- ret_query: bfloat16 [2048, 768], P(None, 'tp'), may hold values from -0.125 to 0.125
- ret_key: bfloat16 [2048, 768], P(None, 'tp'), may hold values from -0.125 to 0.125
- ret_value: bfloat16 [2048, 768], P(None, 'tp'), may hold values from -0.125 to 0.125
- att_query: bfloat16 [2048, 768], P(None, 'tp'), may hold values from -8 to 8
- att_key: bfloat16 [2048, 256], P(None, 'tp'), may hold values from -8 to 8
- att_value: bfloat16 [2048, 256], P(None, 'tp'), may hold values from -0.125 to 0.125
- log_decay: float32 [4, 12, 3072], P('fs', 'tp', 'sp'), may hold values from -1.5 to 0
- ret_gain: float32 [768], P('tp'), may hold values from 0.1 to 1.9
- sink_logit: float32 [12], P('tp'), may hold values from 1 to 5
- retentive_exit_matrix: bfloat16 [768, 2048], P('tp'), may hold values from -0.15625 to 0.15625
- out_att: bfloat16 [768, 2048], P('tp'), may hold values from -0.875 to 0.875
Outputs:
- mixed: bfloat16 [4, 3072, 2048], P('fs', ('sp', 'tp'))
All inputs are finite; a program needn't handle non-finite values.
Results may differ from a plain program's by a relative error of at most 0.0085.
Values may be sent and summed in bfloat16 or wider, within the bound.
A program may use at most 128 MiB of HBM per device.

v0:
```python
import functools

import jax
import jax.numpy as jnp
from jax import lax
from jax.experimental import pallas as pl
from jax.experimental.pallas import tpu as pltpu
from jax.sharding import PartitionSpec as P

HEAD_DIM = 64
WINDOW = 128
CHUNK = 128
LANES = 128
TILE = 256
EXIT_TILE = 512
EPS = 1e-06
F32 = jnp.float32
BF16 = jnp.bfloat16
EXACT = lax.Precision.HIGHEST

NT = (((1,), (1,)), ((), ()))
TN = (((0,), (0,)), ((), ()))


def layer(
    n_sp, n_tp, kv_heads,
    tok, gain_in, rq, rk, rv, aq, ak, av, ld_in, rgain, sink, wr, wa,
    out,
    xb, wb, acc, pb, inv, ldp, ct, cr, eq, ek, dm, st, ub, msg, inbox,
    hb, hin, wo, oacc,
    gain, ld, small_sem, tok_sem, w_sem, wo_sem, x_send, x_recv, wo_send, wo_recv,
    h_send, h_recv, m_send, m_recv, halo_send, halo_recv,
):
    tp = lax.axis_index("tp")
    sp = lax.axis_index("sp")
    rows, depth = tok.shape
    ret_w, att_w, kv_w = rq.shape[1], aq.shape[1], ak.shape[1]
    heads = ld_in.shape[0]
    chunks = rows // CHUNK
    pairs = ret_w // LANES
    att_pairs = att_w // LANES
    att_heads = att_w // HEAD_DIM
    out_rows = rows // n_tp
    model = depth * n_tp
    scale = HEAD_DIM ** (-0.5)

    c_rk, c_rv, c_ak = 0, ret_w, 2 * ret_w
    c_av = c_ak + kv_w
    c_rq = c_av + kv_w
    c_aq = c_rq + ret_w
    width = c_aq + att_w
    parts = ((rk, c_rk), (rv, c_rv), (ak, c_ak), (av, c_av), (rq, c_rq), (aq, c_aq))
    kv_tiles, tiles = c_rq // TILE, width // TILE

    def load_tokens():
        return pltpu.make_async_copy(tok, xb.at[0], tok_sem)

    def load_weight(phase, i):
        owner = lax.rem(tp + phase, n_tp)
        ref, col = parts[i]
        return pltpu.make_async_copy(
            ref.at[pl.ds(owner * depth, depth), :],
            wb.at[phase, :, pl.ds(col, ref.shape[1])],
            w_sem.at[phase, i],
        )

    def load_exit(i):
        ref = (wr, wa)[i]
        return pltpu.make_async_copy(
            ref, wo.at[0, pl.ds(i * ret_w, ref.shape[0]), :], wo_sem.at[i]
        )

    def send_tokens(q):
        return pltpu.make_async_remote_copy(
            src_ref=tok, dst_ref=xb.at[n_tp - q],
            send_sem=x_send.at[q - 1], recv_sem=x_recv.at[n_tp - q - 1],
            device_id={"tp": lax.rem(tp + q, n_tp)}, device_id_type=pl.DeviceIdType.MESH,
        )

    def send_exit(q, i):
        ref = (wr, wa)[i]
        return pltpu.make_async_remote_copy(
            src_ref=ref, dst_ref=wo.at[n_tp - q, pl.ds(i * ret_w, ref.shape[0]), :],
            send_sem=wo_send.at[q - 1, i], recv_sem=wo_recv.at[n_tp - q - 1, i],
            device_id={"tp": lax.rem(tp + q, n_tp)}, device_id_type=pl.DeviceIdType.MESH,
        )

    def send_heads(q, i):
        target = lax.rem(tp + q, n_tp)
        cols = pl.ds(i * ret_w, (ret_w, att_w)[i])
        return pltpu.make_async_remote_copy(
            src_ref=hb.at[pl.ds(target * out_rows, out_rows), cols],
            dst_ref=hin.at[n_tp - q - 1, :, cols],
            send_sem=h_send.at[q - 1, i], recv_sem=h_recv.at[n_tp - q - 1, i],
            device_id={"tp": target}, device_id_type=pl.DeviceIdType.MESH,
        )

    def send_state(q):
        return pltpu.make_async_remote_copy(
            src_ref=msg, dst_ref=inbox.at[q - 1],
            send_sem=m_send.at[q - 1], recv_sem=m_recv.at[q - 1],
            device_id={"sp": lax.rem(sp + q, n_sp)}, device_id_type=pl.DeviceIdType.MESH,
        )

    def send_halo():
        cols = pl.ds(c_ak, 2 * kv_w)
        return pltpu.make_async_remote_copy(
            src_ref=pb.at[pl.ds(rows, WINDOW), cols],
            dst_ref=pb.at[pl.ds(0, WINDOW), cols],
            send_sem=halo_send, recv_sem=halo_recv,
            device_id={"sp": lax.rem(sp + 1, n_sp)}, device_id_type=pl.DeviceIdType.MESH,
        )

    rates = pltpu.make_async_copy(ld_in, ld, small_sem.at[0])
    gains = pltpu.make_async_copy(gain_in, gain, small_sem.at[1])
    rates.start()
    gains.start()
    barrier = pltpu.get_barrier_semaphore()
    for q in range(1, n_tp):
        pl.semaphore_signal(
            barrier, inc=1, device_id={"tp": lax.rem(tp + q, n_tp)},
            device_id_type=pl.DeviceIdType.MESH,
        )
    for q in range(1, n_sp):
        pl.semaphore_signal(
            barrier, inc=1, device_id={"sp": lax.rem(sp + q, n_sp)},
            device_id_type=pl.DeviceIdType.MESH,
        )
    load_tokens().start()
    for phase in range(n_tp):
        for i in range(len(parts)):
            load_weight(phase, i).start()

    lane = lax.broadcasted_iota(jnp.int32, (CHUNK, LANES), 1)
    row = lax.broadcasted_iota(jnp.int32, (CHUNK, LANES), 0)
    first_half = lane < HEAD_DIM
    lane1 = lax.broadcasted_iota(jnp.int32, (1, LANES), 1)
    half_masks = (
        jnp.where(lane1 < HEAD_DIM, 1.0, 0.0).astype(BF16),
        jnp.where(lane1 < HEAD_DIM, 0.0, 1.0).astype(BF16),
    )
    same_head = (row < HEAD_DIM) == first_half
    pad_rows = 8

    tri = jnp.where(lane <= row, 1.0, 0.0).astype(F32)
    ldp[...] = jnp.zeros_like(ldp)
    rates.wait()
    for h in range(heads):
        ldp[h : h + 1, :] = ld[h]

    for c in range(chunks):
        span = slice(c * CHUNK, (c + 1) * CHUNK)
        part = ldp[:, span]
        ct[span, :] = lax.dot_general(
            tri, part, NT, precision=EXACT, preferred_element_type=F32
        )
        cr[c] = lax.dot_general(
            part[:pad_rows], tri, NT, precision=EXACT, preferred_element_type=F32
        )

    def decays(c, carry):
        span = pl.ds(pl.multiple_of(c * CHUNK, CHUNK), CHUNK)
        columns = ct[span, :]
        rows_c = cr[c]
        for p in range(pairs):
            wide = [
                jnp.broadcast_to(columns[:, h : h + 1], (CHUNK, LANES))
                for h in (2 * p, 2 * p + 1)
            ]
            mixed = jnp.where(first_half, wide[0], wide[1])
            cols = slice(p * LANES, (p + 1) * LANES)
            eq[span, cols] = jnp.exp(mixed)
            ek[span, cols] = jnp.exp(mixed[CHUNK - 1 :, :] - mixed) * scale
            for e in range(2):
                h = 2 * p + e
                gap = jnp.where(lane <= row, wide[e] - rows_c[h : h + 1, :], -jnp.inf)
                dm[c, h] = jnp.exp(gap) * scale
        return carry

    lax.fori_loop(0, chunks, decays, 0)

    pl.semaphore_wait(barrier, n_tp - 1 + n_sp - 1)
    for q in range(1, n_tp):
        send_tokens(q).start()

    def scaled(phase):
        owner = lax.rem(tp + phase, n_tp)
        factors = gain[owner]

        def one(i, carry):
            span = pl.ds(pl.multiple_of(i * CHUNK, CHUNK), CHUNK)
            x = xb[phase, span, :].astype(F32)
            xb[phase, span, :] = (x * factors).astype(BF16)
            squares = jnp.broadcast_to(
                jnp.sum(x * x, axis=1, keepdims=True), (CHUNK, LANES)
            )
            if phase > 0:
                squares = inv[span, :] + squares
            if phase == n_tp - 1:
                squares = lax.rsqrt(squares / model + EPS)
            inv[span, :] = squares
            return carry

        lax.fori_loop(0, chunks, one, 0)

    def project(phase, low, high):
        def one(n, carry):
            cols = pl.ds(pl.multiple_of(n * TILE, TILE), TILE)
            total = jnp.dot(xb[phase], wb[phase, :, cols], preferred_element_type=F32)
            if phase > 0:
                total = acc[:, cols] + total
            if phase == n_tp - 1:
                wide = jnp.concatenate([inv[...]] * (TILE // LANES), axis=1)
                pb[WINDOW:, cols] = (total * wide).astype(BF16)
            else:
                acc[:, cols] = total
            return carry

        lax.fori_loop(low, high, one, 0)

    gains.wait()
    load_tokens().wait()
    scaled(0)
    for i in range(4):
        load_weight(0, i).wait()
    project(0, 0, kv_tiles)
    for i in range(4, 6):
        load_weight(0, i).wait()
    for q in range(1, n_tp):
        for i in range(2):
            send_exit(q, i).start()
    for i in range(2):
        load_exit(i).start()
    project(0, kv_tiles, tiles)
    for phase in range(1, n_tp):
        for i in range(6):
            load_weight(phase, i).wait()
        send_tokens(n_tp - phase).wait_recv()
        scaled(phase)
        if phase < n_tp - 1:
            project(phase, 0, tiles)
    project(n_tp - 1, 0, kv_tiles)

    @pl.when(sp + 1 < n_sp)
    def _():
        send_halo().start()

    st[...] = jnp.zeros_like(st)

    def own_state(c, totals):
        span = pl.ds(pl.multiple_of(c * CHUNK, CHUNK), CHUNK)
        here = pl.ds(pl.multiple_of(WINDOW + c * CHUNK, CHUNK), CHUNK)
        after = []
        for p in range(pairs):
            cols = slice(p * LANES, (p + 1) * LANES)
            keys = pb[here, c_rk + p * LANES : c_rk + (p + 1) * LANES].astype(F32)
            values = pb[here, c_rv + p * LANES : c_rv + (p + 1) * LANES]
            keyed = (keys * ek[span, cols]).astype(BF16)
            added = lax.dot_general(keyed, values, TN, preferred_element_type=F32)
            added = jnp.where(same_head, added, 0.0)
            ub[c, p] = added
            fade = eq[span, cols][CHUNK - 1 :, :]
            st[p] = st[p] * fade + added
            after.append(totals[p] * fade)
        return tuple(after)

    totals = lax.fori_loop(
        0, chunks, own_state, tuple(jnp.ones((1, LANES), F32) for _ in range(pairs)),
        unroll=2,
    )
    for p in range(pairs):
        msg[p, :HEAD_DIM, :] = (st[p, :HEAD_DIM, :] + st[p, HEAD_DIM:, :]).astype(BF16)
        coarse = totals[p].astype(BF16)
        fine = (totals[p] - coarse.astype(F32)).astype(BF16)
        row16 = lax.broadcasted_iota(jnp.int32, (16, LANES), 0)
        msg[p, HEAD_DIM:, :] = jnp.where(
            row16 == 0, coarse.astype(F32), jnp.where(row16 == 1, fine.astype(F32), 0.0)
        ).astype(BF16)

    for q in range(1, n_sp):
        @pl.when(sp + q < n_sp)
        def _():
            send_state(q).start()

    project(n_tp - 1, kv_tiles, tiles)

    blocks = rows // WINDOW
    q_at = lax.broadcasted_iota(jnp.int32, (WINDOW, 2 * WINDOW), 0)
    k_at = lax.broadcasted_iota(jnp.int32, (WINDOW, 2 * WINDOW), 1)
    distance = WINDOW + q_at - k_at
    in_window = (distance >= 0) & (distance < WINDOW)

    def attend(i, carry):
        n = blocks - 1 - i

        lowest = jnp.where((n == 0) & (sp == 0), WINDOW, 0)
        allowed = in_window & (k_at >= lowest)
        band = pl.ds(pl.multiple_of(n * WINDOW, WINDOW), 2 * WINDOW)
        here = pl.ds(pl.multiple_of((n + 1) * WINDOW, WINDOW), WINDOW)
        store = pl.ds(pl.multiple_of(n * WINDOW, WINDOW), WINDOW)
        kinds = {}
        for t in range(kv_w // LANES):
            for name, col in (("k", c_ak), ("v", c_av)):
                plain = pb[band, col + t * LANES : col + (t + 1) * LANES]
                turned = pltpu.roll(plain.astype(F32), HEAD_DIM, 1).astype(BF16)
                kinds[name, t] = (plain, turned)
        scores = []
        picks = []
        for h in range(att_heads):
            p, e = h // 2, h % 2
            g = h * kv_heads // att_heads
            picks.append((g // 2, int(g % 2 != e)))
            query = pb[here, c_aq + p * LANES : c_aq + (p + 1) * LANES] * half_masks[e]
            t, turn = picks[h]
            scores.append(
                lax.dot_general(query, kinds["k", t][turn], NT, preferred_element_type=F32)
            )
        weights = []
        for h in range(att_heads):
            s = jnp.where(allowed, scores[h] * scale, -jnp.inf)
            sink_h = sink[h]
            highest = jnp.maximum(jnp.max(s, axis=1, keepdims=True), sink_h)
            raised = jnp.exp(s - highest)
            total = jnp.sum(raised, axis=1, keepdims=True) + jnp.exp(sink_h - highest)
            weights.append((raised * (1.0 / total)).astype(BF16))
        for p in range(att_pairs):
            left = jnp.concatenate([weights[2 * p], weights[2 * p + 1]], axis=1)
            right = jnp.concatenate(
                [
                    kinds["v", picks[2 * p + e][0]][picks[2 * p + e][1]] * half_masks[e]
                    for e in range(2)
                ],
                axis=0,
            )
            hb[store, ret_w + p * LANES : ret_w + (p + 1) * LANES] = jnp.dot(
                left, right, preferred_element_type=F32
            ).astype(BF16)
        return carry

    lax.fori_loop(0, blocks - 1, attend, 0)

    @pl.when(sp > 0)
    def _():
        send_halo().wait_recv()

    @pl.when(sp == 0)
    def _():
        pb[:WINDOW, c_ak : c_ak + 2 * kv_w] = jnp.zeros((WINDOW, 2 * kv_w), BF16)

    lax.fori_loop(blocks - 1, blocks, attend, 0)
    for q in range(1, n_tp):
        send_heads(q, 1).start()

    st[...] = jnp.zeros_like(st)
    for q in range(n_sp - 1, 0, -1):
        @pl.when(sp >= q)
        def _():
            send_state(q).wait_recv()
            for p in range(pairs):
                part = inbox[q - 1, p].astype(F32)
                fade = part[HEAD_DIM : HEAD_DIM + 1] + part[HEAD_DIM + 1 : HEAD_DIM + 2]
                both = jnp.concatenate([part[:HEAD_DIM]] * 2, axis=0)
                st[p] = st[p] * fade + jnp.where(same_head, both, 0.0)

    ones = jnp.where(same_head, 1.0, 0.0).astype(BF16)
    ones2 = jnp.concatenate([ones, ones], axis=0)

    def retain(c, carry):
        span = pl.ds(pl.multiple_of(c * CHUNK, CHUNK), CHUNK)
        here = pl.ds(pl.multiple_of(WINDOW + c * CHUNK, CHUNK), CHUNK)
        kept = []
        for p in range(pairs):
            cols = slice(p * LANES, (p + 1) * LANES)
            query = pb[here, c_rq + p * LANES : c_rq + (p + 1) * LANES]
            keys = pb[here, c_rk + p * LANES : c_rk + (p + 1) * LANES]
            values = pb[here, c_rv + p * LANES : c_rv + (p + 1) * LANES]
            left = [
                (
                    lax.dot_general(
                        query * half_masks[e], keys, NT, preferred_element_type=F32
                    )
                    * dm[c, 2 * p + e]
                ).astype(BF16)
                for e in range(2)
            ]
            state = st[p]
            faded = eq[span, cols]
            left.append((query.astype(F32) * faded).astype(BF16))
            right = [values * half_masks[0], values * half_masks[1], state.astype(BF16)]
            kept.append(
                jnp.dot(
                    jnp.concatenate(left, axis=1),
                    jnp.concatenate(right, axis=0),
                    preferred_element_type=F32,
                )
            )
            st[p] = state * faded[CHUNK - 1 :, :] + ub[c, p]
        for p in range(pairs):
            cols = slice(p * LANES, (p + 1) * LANES)
            r = kept[p]
            square = r * r
            coarse = square.astype(BF16)
            fine = (square - coarse.astype(F32)).astype(BF16)
            total = jnp.dot(
                jnp.concatenate([coarse, fine], axis=1), ones2, preferred_element_type=F32
            )
            normed = r * lax.rsqrt(total * (1.0 / HEAD_DIM) + EPS)
            hb[span, cols] = (normed * rgain[cols].reshape(1, LANES)).astype(BF16)
        return carry

    lax.fori_loop(0, chunks, retain, 0, unroll=2)
    for q in range(1, n_tp):
        send_heads(q, 0).start()

    for i in range(2):
        load_exit(i).wait()
    mine = pl.ds(pl.multiple_of(tp * out_rows, out_rows), out_rows)

    def leave(phase):
        def one(n, carry):
            cols = pl.ds(pl.multiple_of(n * EXIT_TILE, EXIT_TILE), EXIT_TILE)
            left = hb[mine, :] if phase == 0 else hin[phase - 1]
            total = jnp.dot(left, wo[phase, :, cols], preferred_element_type=F32)
            if phase > 0:
                total = oacc[:, cols] + total
            if phase == n_tp - 1:
                out[:, cols] = total.astype(BF16)
            else:
                oacc[:, cols] = total
            return carry

        lax.fori_loop(0, model // EXIT_TILE, one, 0)

    leave(0)
    for phase in range(1, n_tp):
        for i in range(2):
            send_exit(n_tp - phase, i).wait_recv()
            send_heads(n_tp - phase, i).wait_recv()
        leave(phase)

    for q in range(1, n_tp):
        send_tokens(q).wait_send()
        for i in range(2):
            send_exit(q, i).wait_send()
            send_heads(q, i).wait_send()
    for q in range(1, n_sp):
        @pl.when(sp + q < n_sp)
        def _():
            send_state(q).wait_send()

    @pl.when(sp + 1 < n_sp)
    def _():
        send_halo().wait_send()


def shards(n_sp, n_tp, tokens, in_gain, rq, rk, rv, aq, ak, av, log_decay, ret_gain, sink, wr, wa):
    rows, depth = tokens.shape[1:]
    ret_w, att_w, kv_w = rq.shape[1], aq.shape[1], ak.shape[1]
    heads = log_decay.shape[1]
    model = depth * n_tp
    width = 3 * ret_w + att_w + 2 * kv_w
    chunks, pairs = rows // CHUNK, ret_w // LANES
    out_rows = rows // n_tp
    kv_heads = kv_w // HEAD_DIM
    later = max(n_sp - 1, 1)
    others = max(n_tp - 1, 1)
    vmem = pl.BlockSpec(memory_space=pltpu.VMEM)
    hbm = pl.BlockSpec(memory_space=pltpu.HBM)
    smem = pl.BlockSpec(memory_space=pltpu.SMEM)
    dma = pltpu.SemaphoreType.DMA
    result = pl.pallas_call(
        functools.partial(layer, n_sp, n_tp, kv_heads),
        out_shape=pltpu.VMEM((out_rows, model), BF16),
        in_specs=[hbm] * 9 + [vmem, smem, hbm, hbm],
        out_specs=vmem,
        scratch_shapes=[
            pltpu.VMEM((n_tp, rows, depth), BF16),
            pltpu.VMEM((n_tp, depth, width), BF16),
            pltpu.VMEM((rows, width), F32),
            pltpu.VMEM((WINDOW + rows, width), BF16),
            pltpu.VMEM((rows, LANES), F32),
            pltpu.VMEM((LANES, rows), F32),
            pltpu.VMEM((rows, LANES), F32),
            pltpu.VMEM((chunks, 8, CHUNK), F32),
            pltpu.VMEM((rows, ret_w), F32),
            pltpu.VMEM((rows, ret_w), F32),
            pltpu.VMEM((chunks, heads, CHUNK, CHUNK), F32),
            pltpu.VMEM((pairs, LANES, LANES), F32),
            pltpu.VMEM((chunks, pairs, LANES, LANES), F32),
            pltpu.VMEM((pairs, HEAD_DIM + 16, LANES), BF16),
            pltpu.VMEM((later, pairs, HEAD_DIM + 16, LANES), BF16),
            pltpu.VMEM((rows, ret_w + att_w), BF16),
            pltpu.VMEM((others, out_rows, ret_w + att_w), BF16),
            pltpu.VMEM((n_tp, ret_w + att_w, model), BF16),
            pltpu.VMEM((out_rows, model), F32),
            pltpu.VMEM((n_tp, 1, depth), F32),
            pltpu.VMEM((heads, 1, rows), F32),
            dma((2,)),
            dma, dma((n_tp, 6)), dma((2,)),
            dma((others,)), dma((others,)),
            dma((others, 2)), dma((others, 2)),
            dma((others, 2)), dma((others, 2)),
            dma((later,)), dma((later,)),
            dma, dma,
        ],
        compiler_params=pltpu.CompilerParams(
            collective_id=0, has_side_effects=True, vmem_limit_bytes=52 * 1024 * 1024
        ),
    )(
        tokens[0], in_gain.reshape(n_tp, 1, depth), rq, rk, rv, aq, ak, av,
        jnp.transpose(log_decay, (1, 0, 2)), ret_gain, sink, wr, wa,
    )
    return result[None]


def solution(mesh):
    n_sp, n_tp = mesh.shape["sp"], mesh.shape["tp"]
    return jax.shard_map(
        functools.partial(shards, n_sp, n_tp),
        mesh=mesh,
        in_specs=(
            P("fs", "sp", "tp"),
            P(),
            P(None, "tp"),
            P(None, "tp"),
            P(None, "tp"),
            P(None, "tp"),
            P(None, "tp"),
            P(None, "tp"),
            P("fs", "tp", "sp"),
            P("tp"),
            P("tp"),
            P("tp", None),
            P("tp", None),
        ),
        out_specs=P("fs", ("sp", "tp"), None),
        check_vma=False,
    )
```

profile of v0, /device:TPU:0, one launch (start us, length us, event | category | flops | bytes accessed | tf_op | source)
XLA Modules:
  0.0 33.0 jit_solution(16854446406742585682)
XLA Ops:
  0.0 0.0 copy-start
  0.0 0.7 %copy-done = f32[1,6,768]{2,0,1:T(1,128)S(1)} copy-done((f32[1,6,768]{2,0,1:T(1,128)S(1)}, f32[1,6,768]{2,0,1:T(1,128)}, u32[]{:S(2)}) %copy-start) | copy-done | bytes 18456
  0.7 0.0 copy-start.1
  0.7 0.7 %copy-done.1 = f32[2048]{0:T(1024)S(1)} copy-done((f32[2048]{0:T(1024)S(1)}, f32[2048]{0:T(1024)}, u32[]{:S(2)}) %copy-start.1) | copy-done | bytes 8216
  1.4 0.0 copy-start.2
  1.4 0.7 %copy-done.2 = f32[384]{0:T(512)S(1)} copy-done((f32[384]{0:T(512)S(1)}, f32[384]{0:T(512)}, u32[]{:S(2)}) %copy-start.2) | copy-done | bytes 1560
  2.1 0.0 copy-start.3
  2.1 0.7 %copy-done.3 = f32[6]{0:T(128)S(1)} copy-done((f32[6]{0:T(128)S(1)}, f32[6]{0:T(128)}, u32[]{:S(2)}) %copy-start.3) | copy-done | bytes 48
  2.8 29.1 %shard_map.127 = bf16[384,2048]{1,0:T(8,128)(2,1)S(1)} custom-call(bf16[768,1024]{1,0:T(8,128)(2,1)} %bitcast.7, f32[2,1,1024]{2,1,0:T(1,128)S(1)} %bitcast.6, bf16[2048,384]{1,0:T(8,128)(2,1)} %rq.1, bf16[2048,384]{1,0:T(8,128)(2,1)} %rk.1, bf16[2048,384]{1,0:T(8,128)(2,1)} %rv.1, bf16[2048,384]{1,0:T(8,128)(2,1)} %aq.1, bf16[2048,128]{1,0:T(8,128)(2,1)} %ak.1, ...), custom_call_target="tpu_custom_call" | custom-call | tf_op jit(solution)/shard_map/pallas_call | solution.py:471
  31.9 1.1 %copy.15 = bf16[1,384,2048]{2,1,0:T(8,128)(2,1)} copy(bf16[1,384,2048]{2,1,0:T(8,128)(2,1)S(1)} %bitcast.4) | data formatting | bytes 3145728
Async XLA Ops:
  0.0 0.7 %copy-start = (f32[1,6,768]{2,0,1:T(1,128)S(1)}, f32[1,6,768]{2,0,1:T(1,128)}, u32[]{:S(2)}) copy-start(f32[1,6,768]{2,0,1:T(1,128)} %param.21) | copy-start | bytes 55300
  0.7 0.7 %copy-start.1 = (f32[2048]{0:T(1024)S(1)}, f32[2048]{0:T(1024)}, u32[]{:S(2)}) copy-start(f32[2048]{0:T(1024)} %param.14) | copy-start | bytes 24580
  1.4 0.7 %copy-start.2 = (f32[384]{0:T(512)S(1)}, f32[384]{0:T(512)}, u32[]{:S(2)}) copy-start(f32[384]{0:T(512)} %rgain.1) | copy-start | bytes 4612
  2.1 0.7 %copy-start.3 = (f32[6]{0:T(128)S(1)}, f32[6]{0:T(128)}, u32[]{:S(2)}) copy-start(f32[6]{0:T(128)} %sink.1) | copy-start | bytes 76
where the time goes:
time: 33.3 us; the launch traced here: 33 us
  Pallas kernels  29.1 us (87%)
  local copies, waits for them, and re-layouts  3.9 us (12%)
    pallas_call x1, Pallas kernels, shards(): pl.pallas_call(functools.partial(layer, n_sp, n_tp, kv_heads), out_shape=...  29.1 us
    unnamed x9, local copies, waits for them, and re-layouts  3.9 us

commit v1 on v0

v1 whole, which is shorter than its diff:
```python
import functools

import jax
import jax.numpy as jnp
from jax import lax
from jax.experimental import pallas as pl
from jax.experimental.pallas import tpu as pltpu
from jax.sharding import PartitionSpec as P

HEAD_DIM = 64
WINDOW = 128
CHUNK = 128
LANES = 128
TILE = 256
EPS = 1e-06
F32 = jnp.float32
BF16 = jnp.bfloat16

NT = (((1,), (1,)), ((), ()))
TN = (((0,), (0,)), ((), ()))


def weave(*streams):
    order = []
    for k, stream in enumerate(streams):
        for i, piece in enumerate(stream):
            order.append(((i + 0.5) / len(stream), k, i, piece))
    for item in sorted(order, key=lambda entry: entry[:3]):
        item[3]()


def layer(
    n_sp, n_tp,
    tok, gain_in, rq, rk, rv, aq, ak, av, ld_in, rgain_in, sink_in, wr, wa,
    out,
    xb, wb, acc, pb, sq, inv, cr, eqr, ekr, dt, vt, ub, st, stb, ri, bias, sc, pw, dn,
    msg, inbox, hb, hin, wo, oacc, gt,
    gain, ld, rgain, sink, small_sem, tok_sem, w_sem, wo_sem, x_send, x_recv, wo_send, wo_recv,
    h_send, h_recv, m_send, m_recv, halo_send, halo_recv,
):
    tp = lax.axis_index("tp")
    sp = lax.axis_index("sp")
    rows, depth = tok.shape
    ret_w, att_w, kv_w = rq.shape[1], aq.shape[1], ak.shape[1]
    heads = ld_in.shape[0]
    chunks = rows // CHUNK
    pairs = ret_w // LANES
    att_pairs = att_w // LANES
    att_heads = att_w // HEAD_DIM
    kv_heads = kv_w // HEAD_DIM
    group = att_heads // kv_heads
    out_rows = rows // n_tp
    model = depth * n_tp
    scale = HEAD_DIM ** (-0.5)
    half = rows // 2
    blocks = rows // WINDOW

    c_rk, c_rv, c_ak = 0, ret_w, 2 * ret_w
    c_av = c_ak + kv_w
    c_rq = c_av + kv_w
    c_aq = c_rq + ret_w
    width = c_aq + att_w
    parts = ((rk, c_rk), (rv, c_rv), (ak, c_ak), (av, c_av), (rq, c_rq), (aq, c_aq))
    tiles = width // TILE
    ret_tiles = c_ak // TILE
    kv_tiles = c_rq // TILE

    def load_tokens(i):
        span = pl.ds(i * half, half)
        return pltpu.make_async_copy(tok.at[span, :], xb.at[0, span, :], tok_sem.at[i])

    def load_weight(phase, i):
        owner = lax.rem(tp + phase, n_tp)
        ref, col = parts[i]
        return pltpu.make_async_copy(
            ref.at[pl.ds(owner * depth, depth), :],
            wb.at[phase, :, pl.ds(col, ref.shape[1])],
            w_sem.at[phase, i],
        )

    def load_exit(i):
        ref = (wr, wa)[i]
        return pltpu.make_async_copy(
            ref, wo.at[i, pl.ds(0, ref.shape[0]), :], wo_sem.at[i]
        )

    def send_tokens(q, i):
        span = pl.ds(i * half, half)
        return pltpu.make_async_remote_copy(
            src_ref=tok.at[span, :], dst_ref=xb.at[n_tp - q, span, :],
            send_sem=x_send.at[q - 1, i], recv_sem=x_recv.at[n_tp - q - 1, i],
            device_id={"tp": lax.rem(tp + q, n_tp)}, device_id_type=pl.DeviceIdType.MESH,
        )

    def send_exit(q, i):
        ref = (wr, wa)[i]
        return pltpu.make_async_remote_copy(
            src_ref=ref,
            dst_ref=wo.at[i, pl.ds((n_tp - q) * ref.shape[0], ref.shape[0]), :],
            send_sem=wo_send.at[q - 1, i], recv_sem=wo_recv.at[n_tp - q - 1, i],
            device_id={"tp": lax.rem(tp + q, n_tp)}, device_id_type=pl.DeviceIdType.MESH,
        )

    def send_heads(q, i):
        target = lax.rem(tp + q, n_tp)
        cols = pl.ds(i * ret_w, (ret_w, att_w)[i])
        return pltpu.make_async_remote_copy(
            src_ref=hb.at[pl.ds(target * out_rows, out_rows), cols],
            dst_ref=hin.at[n_tp - q - 1, :, cols],
            send_sem=h_send.at[q - 1, i], recv_sem=h_recv.at[n_tp - q - 1, i],
            device_id={"tp": target}, device_id_type=pl.DeviceIdType.MESH,
        )

    def send_state(q):
        return pltpu.make_async_remote_copy(
            src_ref=msg, dst_ref=inbox.at[q - 1],
            send_sem=m_send.at[q - 1], recv_sem=m_recv.at[q - 1],
            device_id={"sp": lax.rem(sp + q, n_sp)}, device_id_type=pl.DeviceIdType.MESH,
        )

    def send_halo():
        cols = pl.ds(c_ak, 2 * kv_w)
        return pltpu.make_async_remote_copy(
            src_ref=pb.at[pl.ds(rows, WINDOW), cols],
            dst_ref=pb.at[pl.ds(0, WINDOW), cols],
            send_sem=halo_send, recv_sem=halo_recv,
            device_id={"sp": lax.rem(sp + 1, n_sp)}, device_id_type=pl.DeviceIdType.MESH,
        )

    smalls = [
        pltpu.make_async_copy(src, dst, small_sem.at[i])
        for i, (src, dst) in enumerate(
            ((ld_in, ld), (gain_in, gain), (rgain_in, rgain), (sink_in, sink))
        )
    ]
    for copy in smalls:
        copy.start()
    for i in range(2):
        load_tokens(i).start()
    for i in range(2):
        load_weight(0, i).start()
    barrier = pltpu.get_barrier_semaphore()
    for q in range(1, n_tp):
        pl.semaphore_signal(
            barrier, inc=1, device_id={"tp": lax.rem(tp + q, n_tp)},
            device_id_type=pl.DeviceIdType.MESH,
        )
    for q in range(1, n_sp):
        pl.semaphore_signal(
            barrier, inc=1, device_id={"sp": lax.rem(sp + q, n_sp)},
            device_id_type=pl.DeviceIdType.MESH,
        )

    lane1 = lax.broadcasted_iota(jnp.int32, (1, LANES), 1)
    first_lanes = lane1 < HEAD_DIM
    half_masks = (
        jnp.where(first_lanes, scale, 0.0).astype(BF16),
        jnp.where(first_lanes, 0.0, scale).astype(BF16),
    )
    lane = lax.broadcasted_iota(jnp.int32, (CHUNK, LANES), 1)
    row = lax.broadcasted_iota(jnp.int32, (CHUNK, LANES), 0)
    same_head = (row < HEAD_DIM) == (lane < HEAD_DIM)
    k_at = lax.broadcasted_iota(jnp.int32, (2 * WINDOW, WINDOW), 0)
    q_at = lax.broadcasted_iota(jnp.int32, (2 * WINDOW, WINDOW), 1)
    in_window = (k_at > q_at) & (k_at <= q_at + WINDOW)
    bias[0] = jnp.where(in_window, 0.0, -jnp.inf)
    bias[1] = jnp.where(in_window & (k_at >= WINDOW), 0.0, -jnp.inf)

    pad = cr.shape[1]
    cr[...] = jnp.zeros_like(cr)
    for copy in smalls:
        copy.wait()
    for p in range(pairs):
        gt[p] = jnp.broadcast_to(
            rgain[p * LANES : (p + 1) * LANES].reshape(1, LANES), (LANES, LANES)
        ).T
    for h in range(heads):
        for c in range(chunks):
            cr[c, h : h + 1, :] = ld[h, :, c * CHUNK : (c + 1) * CHUNK]
    steps = cr[...].reshape(chunks * pad, CHUNK)
    top = steps.astype(BF16)
    rest = steps - top.astype(F32)
    mid = rest.astype(BF16)
    low = (rest - mid.astype(F32)).astype(BF16)
    upto = jnp.where(row <= lane, 1.0, 0.0).astype(BF16)
    sums = jnp.dot(
        jnp.concatenate([top, mid, low], axis=0), upto, preferred_element_type=F32
    )
    n_steps = chunks * pad
    cumulative = sums[:n_steps] + (sums[n_steps : 2 * n_steps] + sums[2 * n_steps :])
    cr[...] = cumulative.reshape(chunks, pad, CHUNK)
    eqr[...] = jnp.exp(cumulative).reshape(chunks, pad, CHUNK)
    ekr[...] = (jnp.exp(cumulative[:, CHUNK - 1 :] - cumulative) * scale).reshape(
        chunks, pad, CHUNK
    )
    filler = jnp.zeros((LANES - n_steps % LANES, CHUNK), F32)
    columns = jnp.concatenate([cumulative, filler], axis=0).T

    def decay(c, h):
        def piece():
            at = c * pad + h
            wide = jnp.broadcast_to(columns[:, at : at + 1], (CHUNK, LANES))
            gap = jnp.where(row <= lane, cr[c, h : h + 1, :] - wide, -jnp.inf)
            dt[c, h // 2, :, (h % 2) * CHUNK : (h % 2 + 1) * CHUNK] = jnp.exp(gap)

        return piece

    def scaled(phase, i):
        def piece():
            owner = lax.rem(tp + phase, n_tp)
            span = slice(i * CHUNK, (i + 1) * CHUNK)
            x = xb[phase, span, :].astype(F32)
            xb[phase, span, :] = (x * gain[owner]).astype(BF16)
            squares = jnp.broadcast_to(
                jnp.sum(x * x, axis=1, keepdims=True), (CHUNK, LANES)
            )
            if phase > 0:
                squares = sq[span, :] + squares
            if phase == n_tp - 1:
                inv[span, :] = lax.rsqrt(squares / model + EPS)
            else:
                sq[span, :] = squares

        return piece

    def project(phase, n, i, parts_of=2):
        def piece():
            size = rows // parts_of
            cols = slice(n * TILE, (n + 1) * TILE)
            span = slice(i * size, (i + 1) * size)
            total = jnp.dot(
                xb[phase, span, :], wb[phase, :, cols], preferred_element_type=F32
            )
            if phase > 0:
                total = acc[span, cols] + total
            if phase == n_tp - 1:
                wide = jnp.concatenate([inv[span, :]] * (TILE // LANES), axis=1)
                pb[WINDOW + i * size : WINDOW + (i + 1) * size, cols] = (
                    total * wide
                ).astype(BF16)
            else:
                acc[span, cols] = total

        return piece

    per_half = half // CHUNK
    load_tokens(0).wait()
    for i in range(2, 6):
        load_weight(0, i).start()
    weave([scaled(0, i) for i in range(per_half)])
    load_tokens(1).wait()
    for i in range(2):
        load_weight(0, i).wait()
    decays = [decay(c, h) for c in range(chunks) for h in range(heads)]
    weave(
        [project(0, n, 0) for n in range(ret_tiles)],
        [scaled(0, i) for i in range(per_half, chunks)],
    )
    cut = len(decays) // 2
    weave([project(0, n, 1) for n in range(ret_tiles)], decays[:cut])
    pl.semaphore_wait(barrier, n_tp - 1 + n_sp - 1)
    for q in range(1, n_tp):
        for i in range(2):
            send_tokens(q, i).start()
    for phase in range(1, n_tp):
        for i in range(6):
            load_weight(phase, i).start()
    for i in range(2, 6):
        load_weight(0, i).wait()
    weave([project(0, n, 0, 1) for n in range(ret_tiles, tiles)], decays[cut:])
    for q in range(1, n_tp):
        for i in range(1, -1, -1):
            send_exit(q, i).start()
    for i in range(1, -1, -1):
        load_exit(i).start()
    for phase in range(1, n_tp - 1):
        for i in range(2):
            send_tokens(n_tp - phase, i).wait_recv()
        for i in range(6):
            load_weight(phase, i).wait()
        weave([scaled(phase, i) for i in range(chunks)])
        weave([project(phase, n, 0, 1) for n in range(tiles)])
    last = n_tp - 1
    for i in range(6):
        load_weight(last, i).wait()
    send_tokens(n_tp - last, 0).wait_recv()
    weave([scaled(last, i) for i in range(per_half)])
    send_tokens(n_tp - last, 1).wait_recv()

    def here(c):
        return pl.ds(pl.multiple_of(WINDOW + c * CHUNK, CHUNK), CHUNK)

    def own_state(c):
        def piece():
            for p in range(pairs):
                cols = slice(c_rv + p * LANES, c_rv + (p + 1) * LANES)
                turned = pb[here(c), cols].T
                vt[c, p] = turned
                wide = turned.astype(F32)
                faded = jnp.concatenate(
                    [
                        wide[:HEAD_DIM] * ekr[c, 2 * p : 2 * p + 1, :],
                        wide[HEAD_DIM:] * ekr[c, 2 * p + 1 : 2 * p + 2, :],
                    ],
                    axis=0,
                ).astype(BF16)
                keys = pb[here(c), c_rk + p * LANES : c_rk + (p + 1) * LANES]
                added = jnp.dot(faded, keys, preferred_element_type=F32)
                ub[c, p] = jnp.where(same_head, added, 0.0)

        return piece

    def fade_row(c, p):
        ends = [
            jnp.broadcast_to(eqr[c, h : h + 1, CHUNK - 1 :], (1, LANES))
            for h in (2 * p, 2 * p + 1)
        ]
        return jnp.where(first_lanes, ends[0], ends[1])

    weave(
        [project(last, n, 0) for n in range(ret_tiles)],
        [scaled(last, i) for i in range(per_half, chunks)],
    )
    weave(
        [project(last, n, 1) for n in range(ret_tiles)],
        [own_state(c) for c in range(per_half)],
    )
    weave([own_state(c) for c in range(per_half, chunks)])
    totals = []
    for p in range(pairs):
        state = ub[0, p]
        total = fade_row(0, p)
        for c in range(1, chunks):
            fade = fade_row(c, p)
            state = state * fade + ub[c, p]
            total = total * fade
        msg[p * HEAD_DIM : (p + 1) * HEAD_DIM, :] = (
            state[:HEAD_DIM] + state[HEAD_DIM:]
        ).astype(BF16)
        coarse = total.astype(BF16).astype(F32)
        totals += [coarse, total - coarse]
    row16 = lax.broadcasted_iota(jnp.int32, (16, LANES), 0)
    tail = jnp.zeros((16, LANES), F32)
    for i, value in enumerate(totals):
        tail = jnp.where(row16 == i, value, tail)
    msg[pairs * HEAD_DIM :, :] = tail.astype(BF16)
    for q in range(n_sp - 1, 0, -1):
        @pl.when(sp + q < n_sp)
        def _():
            send_state(q).start()

    weave([project(last, n, 0, 1) for n in range(ret_tiles, kv_tiles)])

    @pl.when(sp + 1 < n_sp)
    def _():
        send_halo().start()

    weave([project(last, n, 0, 1) for n in range(tiles - 1, kv_tiles, -1)])

    def score(n):
        def piece(g):
            t, e = g // 2, g % 2
            band = pl.ds(n * WINDOW, 2 * WINDOW)
            keys = pb[band, c_ak + t * LANES : c_ak + (t + 1) * LANES]
            swapped = pltpu.roll(keys.astype(F32), HEAD_DIM, 1).astype(BF16)
            both = jnp.where(first_lanes == (e == 0), keys, swapped)
            queries = []
            for h in range(g * group, (g + 1) * group):
                at = c_aq + (h // 2) * LANES
                queries.append(pb[here(n), at : at + LANES] * half_masks[h % 2])
            sc[n, :, g * group * WINDOW : (g + 1) * group * WINDOW] = lax.dot_general(
                both, jnp.concatenate(queries, axis=0), NT, preferred_element_type=F32
            )

        return [functools.partial(piece, g) for g in range(kv_heads)]

    cut_off = jnp.where(sp == 0, 1, 0)
    step = 32

    def weigh(n):
        def piece(h):
            cols = slice(h * WINDOW, (h + 1) * WINDOW)
            masked = bias.at[cut_off if n == 0 else 0]
            tops = []
            for i in range(2 * WINDOW // step):
                span = slice(i * step, (i + 1) * step)
                s = sc[n, span, cols] + masked[span, :]
                tops.append(jnp.max(s, axis=0, keepdims=True))
            sink_h = jnp.full((1, WINDOW), sink[h], F32)
            top = functools.reduce(jnp.maximum, tops, sink_h)
            dn[n, h : h + 1, :] = jnp.exp(sink_h - top)
            for i in range(2 * WINDOW // step):
                span = slice(i * step, (i + 1) * step)
                s = sc[n, span, cols] + masked[span, :]
                pw[n, span, cols] = jnp.exp(s - top).astype(BF16)

        return [functools.partial(piece, h) for h in range(att_heads)]

    def gather(n):
        def piece():
            band = pl.ds(n * WINDOW, 2 * WINDOW)
            ones = jnp.ones((16, 2 * WINDOW), BF16)
            turned = [
                pb[band, c_av + t * LANES : c_av + (t + 1) * LANES].T
                for t in range(kv_w // LANES)
            ]
            parts_out = []
            for g in range(kv_heads):
                e = g % 2
                left = jnp.concatenate(
                    [turned[g // 2][e * HEAD_DIM : (e + 1) * HEAD_DIM], ones], axis=0
                )
                cols = slice(g * group * WINDOW, (g + 1) * group * WINDOW)
                total = jnp.dot(left, pw[n, :, cols], preferred_element_type=F32)
                for j in range(group):
                    h = g * group + j
                    cols = slice(j * WINDOW, (j + 1) * WINDOW)
                    below = total[HEAD_DIM : HEAD_DIM + 1, cols] + dn[n, h : h + 1, :]
                    parts_out.append((total[:HEAD_DIM, cols] * (1.0 / below)).astype(BF16))
            for p in range(att_pairs):
                hb[n * WINDOW : (n + 1) * WINDOW, ret_w + p * LANES : ret_w + (p + 1) * LANES] = (
                    jnp.concatenate(parts_out[2 * p : 2 * p + 2], axis=0).T
                )

        return [piece]

    order = list(range(blocks - 1, -1, -1))
    rest = [project(last, kv_tiles, i) for i in range(2)]
    for i in range(blocks + 2):
        if i == blocks - 1:
            @pl.when(sp > 0)
            def _():
                send_halo().wait_recv()

            @pl.when(sp == 0)
            def _():
                pb[:WINDOW, c_ak : c_ak + 2 * kv_w] = jnp.zeros((WINDOW, 2 * kv_w), BF16)
        weave(
            score(order[i]) if i < blocks else [],
            weigh(order[i - 1]) if 0 <= i - 1 < blocks else [],
            gather(order[i - 2]) if 0 <= i - 2 < blocks else [],
            [rest.pop()] if rest and i > 0 else [],
        )
    for q in range(1, n_tp):
        send_heads(q, 1).start()

    def intra(c):
        def piece(p):
            query = pb[here(c), c_rq + p * LANES : c_rq + (p + 1) * LANES]
            keys = pb[here(c), c_rk + p * LANES : c_rk + (p + 1) * LANES]
            queries = jnp.concatenate([query * half_masks[e] for e in range(2)], axis=0)
            weights = (
                lax.dot_general(keys, queries, NT, preferred_element_type=F32) * dt[c, p]
            ).astype(BF16)
            total = jnp.dot(vt[c, p], weights, preferred_element_type=F32)
            ri[c, p, :HEAD_DIM, :] = total[:HEAD_DIM, :CHUNK]
            ri[c, p, HEAD_DIM:, :] = total[HEAD_DIM:, CHUNK:]

        return [functools.partial(piece, p) for p in range(pairs)]

    weave([piece for c in range(chunks) for piece in intra(c)])

    st[...] = jnp.zeros_like(st)
    for q in range(n_sp - 1, 0, -1):
        @pl.when(sp >= q)
        def _():
            send_state(q).wait_recv()
            tail = inbox[q - 1, pairs * HEAD_DIM :, :].astype(F32)
            for p in range(pairs):
                part = inbox[q - 1, p * HEAD_DIM : (p + 1) * HEAD_DIM, :].astype(F32)
                fade = tail[2 * p : 2 * p + 1] + tail[2 * p + 1 : 2 * p + 2]
                both = jnp.concatenate([part, part], axis=0)
                st[p] = st[p] * fade + jnp.where(same_head, both, 0.0)

    for p in range(pairs):
        state = st[p]
        for c in range(chunks):
            stb[c, p] = state.astype(BF16)
            if c + 1 < chunks:
                state = state * fade_row(c, p) + ub[c, p]

    mine = pl.ds(pl.multiple_of(tp * out_rows, out_rows), out_rows)
    ranks = n_tp * ret_w

    def leave(kind, n):
        def piece():
            cols = slice(n * TILE, (n + 1) * TILE)
            inner = slice(kind * ret_w, (kind + 1) * ret_w)
            left = jnp.concatenate(
                [hb[mine, inner]] + [hin[phase - 1, :, inner] for phase in range(1, n_tp)],
                axis=1,
            )
            total = jnp.dot(left, wo[kind, :, cols], preferred_element_type=F32)
            if kind == 1:
                oacc[:, cols] = total
            else:
                out[:, cols] = (oacc[:, cols] + total).astype(BF16)

        return piece

    def finish(c):
        def piece(p):
            query = pb[here(c), c_rq + p * LANES : c_rq + (p + 1) * LANES]
            carried = lax.dot_general(stb[c, p], query, NT, preferred_element_type=F32)
            normed = []
            for e in range(2):
                span = slice(e * HEAD_DIM, (e + 1) * HEAD_DIM)
                h = 2 * p + e
                r = ri[c, p, span, :] + carried[span] * eqr[c, h : h + 1, :]
                square = jnp.sum(r * r, axis=0, keepdims=True)
                normed.append(
                    (r * lax.rsqrt(square * (1.0 / HEAD_DIM) + EPS) * gt[p, span, :]).astype(BF16)
                )
            rows_c = pl.ds(pl.multiple_of(c * CHUNK, CHUNK), CHUNK)
            hb[rows_c, p * LANES : (p + 1) * LANES] = jnp.concatenate(normed, axis=0).T

        return [functools.partial(piece, p) for p in range(pairs)]

    for i in range(2):
        load_exit(i).wait()
    for phase in range(1, n_tp):
        for i in range(2):
            send_exit(n_tp - phase, i).wait_recv()
        send_heads(n_tp - phase, 1).wait_recv()
    each = chunks // n_tp
    exits = [leave(1, n) for n in range(model // TILE)]
    share = len(exits) // n_tp
    for q in range(1, n_tp + 1):
        first = lax.rem(tp + q, n_tp) * each
        weave(
            [piece for i in range(each) for piece in finish(first + i)],
            exits[(q - 1) * share : q * share if q < n_tp else len(exits)],
        )
        if q < n_tp:
            send_heads(q, 0).start()
    for phase in range(1, n_tp):
        send_heads(n_tp - phase, 0).wait_recv()
    weave([leave(0, n) for n in range(model // TILE)])
    for q in range(1, n_tp):
        for i in range(2):
            send_tokens(q, i).wait_send()
            send_exit(q, i).wait_send()
            send_heads(q, i).wait_send()
    for q in range(1, n_sp):
        @pl.when(sp + q < n_sp)
        def _():
            send_state(q).wait_send()

    @pl.when(sp + 1 < n_sp)
    def _():
        send_halo().wait_send()


def shards(n_sp, n_tp, tokens, in_gain, rq, rk, rv, aq, ak, av, log_decay, ret_gain, sink, wr, wa):
    rows, depth = tokens.shape[1:]
    ret_w, att_w, kv_w = rq.shape[1], aq.shape[1], ak.shape[1]
    heads = log_decay.shape[1]
    model = depth * n_tp
    width = 3 * ret_w + att_w + 2 * kv_w
    chunks, pairs, blocks = rows // CHUNK, ret_w // LANES, rows // WINDOW
    att_heads = att_w // HEAD_DIM
    out_rows = rows // n_tp
    later = max(n_sp - 1, 1)
    others = max(n_tp - 1, 1)
    packed = pairs * HEAD_DIM + 16
    pad = 8
    hbm = pl.BlockSpec(memory_space=pltpu.HBM)
    dma = pltpu.SemaphoreType.DMA
    result = pl.pallas_call(
        functools.partial(layer, n_sp, n_tp),
        out_shape=pltpu.VMEM((out_rows, model), BF16),
        in_specs=[hbm] * 13,
        out_specs=pl.BlockSpec(memory_space=pltpu.VMEM),
        scratch_shapes=[
            pltpu.VMEM((n_tp, rows, depth), BF16),
            pltpu.VMEM((n_tp, depth, width), BF16),
            pltpu.VMEM((rows, width), F32),
            pltpu.VMEM((WINDOW + rows, width), BF16),
            pltpu.VMEM((rows, LANES), F32),
            pltpu.VMEM((rows, LANES), F32),
            pltpu.VMEM((chunks, pad, CHUNK), F32),
            pltpu.VMEM((chunks, pad, CHUNK), F32),
            pltpu.VMEM((chunks, pad, CHUNK), F32),
            pltpu.VMEM((chunks, pairs, CHUNK, 2 * CHUNK), F32),
            pltpu.VMEM((chunks, pairs, LANES, CHUNK), BF16),
            pltpu.VMEM((chunks, pairs, LANES, LANES), F32),
            pltpu.VMEM((pairs, LANES, LANES), F32),
            pltpu.VMEM((chunks, pairs, LANES, LANES), BF16),
            pltpu.VMEM((chunks, pairs, LANES, CHUNK), F32),
            pltpu.VMEM((2, 2 * WINDOW, WINDOW), F32),
            pltpu.VMEM((blocks, 2 * WINDOW, att_heads * WINDOW), F32),
            pltpu.VMEM((blocks, 2 * WINDOW, att_heads * WINDOW), BF16),
            pltpu.VMEM((blocks, 8, WINDOW), F32),
            pltpu.VMEM((packed, LANES), BF16),
            pltpu.VMEM((later, packed, LANES), BF16),
            pltpu.VMEM((rows, ret_w + att_w), BF16),
            pltpu.VMEM((others, out_rows, ret_w + att_w), BF16),
            pltpu.VMEM((2, n_tp * ret_w, model), BF16),
            pltpu.VMEM((out_rows, model), F32),
            pltpu.VMEM((pairs, LANES, LANES), F32),
            pltpu.VMEM((n_tp, 1, depth), F32),
            pltpu.VMEM((heads, 1, rows), F32),
            pltpu.VMEM((ret_w,), F32),
            pltpu.SMEM(sink.shape, F32),
            dma((4,)), dma((2,)), dma((n_tp, 6)), dma((2,)),
            dma((others, 2)), dma((others, 2)),
            dma((others, 2)), dma((others, 2)),
            dma((others, 2)), dma((others, 2)),
            dma((later,)), dma((later,)),
            dma, dma,
        ],
        compiler_params=pltpu.CompilerParams(
            collective_id=0, has_side_effects=True, vmem_limit_bytes=62 * 1024 * 1024
        ),
    )(
        tokens[0], in_gain.reshape(n_tp, 1, depth), rq, rk, rv, aq, ak, av,
        jnp.transpose(log_decay, (1, 0, 2)), ret_gain, sink, wr, wa,
    )
    return result[None]


def solution(mesh):
    n_sp, n_tp = mesh.shape["sp"], mesh.shape["tp"]
    return jax.shard_map(
        functools.partial(shards, n_sp, n_tp),
        mesh=mesh,
        in_specs=(
            P("fs", "sp", "tp"),
            P(),
            P(None, "tp"),
            P(None, "tp"),
            P(None, "tp"),
            P(None, "tp"),
            P(None, "tp"),
            P(None, "tp"),
            P("fs", "tp", "sp"),
            P("tp"),
            P("tp"),
            P("tp", None),
            P("tp", None),
        ),
        out_specs=P("fs", ("sp", "tp"), None),
        check_vma=False,
    )
```

time: 33.3 us -> 24.4 us (0.73)
  the two profiles are of different devices: /device:TPU:0 before, /device:TPU:19 now
where the time goes in v1:
time: 24.4 us; the launch traced here: 24.3 us
  Pallas kernels  23.1 us (95%)
  local copies, waits for them, and re-layouts  1.15 us (5%)
    pallas_call x1, Pallas kernels, shards(): pl.pallas_call(functools.partial(layer, n_sp, n_tp), out_shape=pltpu.VMEM...  23.1 us
    unnamed x1, local copies, waits for them, and re-layouts  1.15 us

profile of v1, /device:TPU:19, one launch (start us, length us, event | category | flops | bytes accessed | tf_op | source)
XLA Modules:
  0.0 24.3 jit_solution(1601474164939155681)
XLA Ops:
  0.0 23.1 %shard_map.127 = bf16[384,2048]{1,0:T(8,128)(2,1)S(1)} custom-call(bf16[768,1024]{1,0:T(8,128)(2,1)} %bitcast.5, f32[2,1,1024]{2,1,0:T(1,128)} %bitcast.7, bf16[2048,384]{1,0:T(8,128)(2,1)} %rq.1, bf16[2048,384]{1,0:T(8,128)(2,1)} %rk.1, bf16[2048,384]{1,0:T(8,128)(2,1)} %rv.1, bf16[2048,384]{1,0:T(8,128)(2,1)} %aq.1, bf16[2048,128]{1,0:T(8,128)(2,1)} %ak.1, ...), custom_call_target="tpu_custom_call" | custom-call | tf_op jit(solution)/shard_map/pallas_call | solution.py:569
  23.1 1.1 %copy.15 = bf16[1,384,2048]{2,1,0:T(8,128)(2,1)} copy(bf16[1,384,2048]{2,1,0:T(8,128)(2,1)S(1)} %bitcast.4) | data formatting | bytes 3145728

commit v2 on v1

v2 whole, which is shorter than its diff:
```python
import functools

import jax
import jax.numpy as jnp
from jax import lax
from jax.experimental import pallas as pl
from jax.experimental.pallas import tpu as pltpu
from jax.sharding import PartitionSpec as P

HEAD_DIM = 64
WINDOW = 128
CHUNK = 128
LANES = 128
TILE = 256
EPS = 1e-06
F32 = jnp.float32
BF16 = jnp.bfloat16

NT = (((1,), (1,)), ((), ()))
TN = (((0,), (0,)), ((), ()))


def weave(*streams):
    order = []
    for k, stream in enumerate(streams):
        for i, piece in enumerate(stream):
            order.append(((i + 0.5) / len(stream), k, i, piece))
    for item in sorted(order, key=lambda entry: entry[:3]):
        item[3]()


def layer(
    n_sp, n_tp,
    tok, gain_in, rq, rk, rv, aq, ak, av, ld_in, rgain_in, sink_in, wr, wa,
    out,
    xb, wb, acc, pb, sq, inv, cr, eqr, ekr, dt, vt, ub, st, stb, ri, early, kd, va, sc, pw, dn, ao,
    rs, rw, msg, inbox, halo, sr, hb, hin, wo, oacc, gt,
    gain, ld, rgain, sink, small_sem, tok_sem, w_sem, wo_sem, x_send, x_recv, wo_send, wo_recv,
    h_send, h_recv, m_send, m_recv, s_send, s_recv, halo_send, halo_recv, ready,
):
    tp = lax.axis_index("tp")
    sp = lax.axis_index("sp")
    rows, depth = tok.shape
    ret_w, att_w, kv_w = rq.shape[1], aq.shape[1], ak.shape[1]
    heads = ld_in.shape[0]
    chunks = rows // CHUNK
    pairs = ret_w // LANES
    att_pairs = att_w // LANES
    att_heads = att_w // HEAD_DIM
    kv_heads = kv_w // HEAD_DIM
    group = att_heads // kv_heads
    out_rows = rows // n_tp
    model = depth * n_tp
    scale = HEAD_DIM ** (-0.5)
    half = rows // 2
    blocks = rows // WINDOW

    c_ak, c_av = 0, kv_w
    c_pairs = 2 * kv_w
    c_aq = c_pairs + 2 * ret_w
    c_rq = c_aq + att_w
    width = c_rq + ret_w
    parts = [(ak, 0, kv_w, c_ak), (av, 0, kv_w, c_av)]
    for p in range(pairs):
        parts.append((rk, p * LANES, LANES, c_pairs + p * 2 * LANES))
        parts.append((rv, p * LANES, LANES, c_pairs + p * 2 * LANES + LANES))
    parts += [(aq, 0, att_w, c_aq), (rq, 0, ret_w, c_rq)]
    pair_tiles = [
        slice(c_pairs + p * 2 * LANES, c_pairs + (p + 1) * 2 * LANES) for p in range(pairs)
    ]
    kv_tile = slice(c_ak, c_pairs)
    query_tiles = [slice(at, at + TILE) for at in range(c_aq, width, TILE)]

    def c_rk(p):
        return slice(c_pairs + p * 2 * LANES, c_pairs + p * 2 * LANES + LANES)

    def c_rv(p):
        return slice(c_pairs + p * 2 * LANES + LANES, c_pairs + (p + 1) * 2 * LANES)

    def load_tokens(i):
        span = pl.ds(i * half, half)
        return pltpu.make_async_copy(tok.at[span, :], xb.at[0, span, :], tok_sem.at[i])

    def load_weight(phase, i):
        owner = lax.rem(tp + phase, n_tp)
        ref, at, size, col = parts[i]
        return pltpu.make_async_copy(
            ref.at[pl.ds(owner * depth, depth), pl.ds(at, size)],
            wb.at[phase, :, pl.ds(col, size)],
            w_sem.at[phase + 1 if phase > 0 or i >= 4 else 0],
        )

    def wait_weights(group):
        cut = c_pairs + 2 * LANES
        ref = wb.at[max(group - 1, 0)]
        if group < 2:
            ref = ref.at[:, pl.ds(0, cut) if group == 0 else pl.ds(cut, width - cut)]
        pltpu.make_async_copy(ref, ref, w_sem.at[group]).wait()

    def load_exit(i):
        ref = (wr, wa)[i]
        return pltpu.make_async_copy(
            ref, wo.at[i, pl.ds(0, ref.shape[0]), :], wo_sem
        )

    def wait_exit():
        ref = wo.at[:, pl.ds(0, ret_w), :]
        pltpu.make_async_copy(ref, ref, wo_sem).wait()

    def all_tokens(q):
        return pltpu.make_async_remote_copy(
            src_ref=xb.at[0], dst_ref=xb.at[n_tp - q],
            send_sem=x_send.at[q - 1], recv_sem=x_recv.at[n_tp - q - 1],
            device_id={"tp": lax.rem(tp + q, n_tp)}, device_id_type=pl.DeviceIdType.MESH,
        )

    def all_exit(q):
        here_ = wo.at[:, pl.ds((n_tp - q) * ret_w, ret_w), :]
        return pltpu.make_async_remote_copy(
            src_ref=here_, dst_ref=here_,
            send_sem=wo_send.at[q - 1], recv_sem=wo_recv.at[n_tp - q - 1],
            device_id={"tp": lax.rem(tp + q, n_tp)}, device_id_type=pl.DeviceIdType.MESH,
        )

    def all_heads(q):
        target = lax.rem(tp + q, n_tp)
        return pltpu.make_async_remote_copy(
            src_ref=hb.at[pl.ds(target * out_rows, out_rows), :],
            dst_ref=hin.at[n_tp - q - 1],
            send_sem=h_send.at[q - 1], recv_sem=h_recv.at[n_tp - q - 1, 0],
            device_id={"tp": target}, device_id_type=pl.DeviceIdType.MESH,
        )

    def all_states(q):
        return pltpu.make_async_remote_copy(
            src_ref=msg, dst_ref=inbox.at[q - 1],
            send_sem=m_send.at[q - 1], recv_sem=m_recv.at[q - 1],
            device_id={"sp": lax.rem(sp + q, n_sp)}, device_id_type=pl.DeviceIdType.MESH,
        )

    def send_tokens(q, i):
        span = pl.ds(i * half, half)
        return pltpu.make_async_remote_copy(
            src_ref=xb.at[0, span, :], dst_ref=xb.at[n_tp - q, span, :],
            send_sem=x_send.at[q - 1], recv_sem=x_recv.at[n_tp - q - 1],
            device_id={"tp": lax.rem(tp + q, n_tp)}, device_id_type=pl.DeviceIdType.MESH,
        )

    def send_squares(q):
        return pltpu.make_async_remote_copy(
            src_ref=sr.at[0], dst_ref=sr.at[n_tp - q],
            send_sem=s_send.at[q - 1], recv_sem=s_recv.at[n_tp - q - 1],
            device_id={"tp": lax.rem(tp + q, n_tp)}, device_id_type=pl.DeviceIdType.MESH,
        )

    def send_exit(q, i):
        ref = (wr, wa)[i]
        return pltpu.make_async_remote_copy(
            src_ref=ref,
            dst_ref=wo.at[i, pl.ds((n_tp - q) * ref.shape[0], ref.shape[0]), :],
            send_sem=wo_send.at[q - 1], recv_sem=wo_recv.at[n_tp - q - 1],
            device_id={"tp": lax.rem(tp + q, n_tp)}, device_id_type=pl.DeviceIdType.MESH,
        )

    def send_heads(q, i):
        target = lax.rem(tp + q, n_tp)
        cols = pl.ds(i * ret_w, (ret_w, att_w)[i])
        return pltpu.make_async_remote_copy(
            src_ref=hb.at[pl.ds(target * out_rows, out_rows), cols],
            dst_ref=hin.at[n_tp - q - 1, :, cols],
            send_sem=h_send.at[q - 1], recv_sem=h_recv.at[n_tp - q - 1, i],
            device_id={"tp": target}, device_id_type=pl.DeviceIdType.MESH,
        )

    def send_state(q, p):
        span = pl.ds(0, 16 + HEAD_DIM) if p == 0 else pl.ds(16 + p * HEAD_DIM, HEAD_DIM)
        return pltpu.make_async_remote_copy(
            src_ref=msg.at[span, :], dst_ref=inbox.at[q - 1, span, :],
            send_sem=m_send.at[q - 1], recv_sem=m_recv.at[q - 1],
            device_id={"sp": lax.rem(sp + q, n_sp)}, device_id_type=pl.DeviceIdType.MESH,
        )

    def send_halo():
        cols = pl.ds(c_ak, 2 * kv_w)
        return pltpu.make_async_remote_copy(
            src_ref=pb.at[pl.ds(rows, WINDOW), cols],
            dst_ref=halo,
            send_sem=halo_send, recv_sem=halo_recv,
            device_id={"sp": lax.rem(sp + 1, n_sp)}, device_id_type=pl.DeviceIdType.MESH,
        )

    smalls = [
        pltpu.make_async_copy(src, dst, small_sem.at[i])
        for i, (src, dst) in enumerate(
            ((ld_in, ld), (gain_in, gain), (rgain_in, rgain), (sink_in, sink))
        )
    ]
    for copy in smalls:
        copy.start()
    barrier = pltpu.get_barrier_semaphore()
    for q in range(1, n_tp):
        pl.semaphore_signal(
            barrier, inc=1, device_id={"tp": lax.rem(tp + q, n_tp)},
            device_id_type=pl.DeviceIdType.MESH,
        )
    for q in range(1, n_sp):
        @pl.when(sp + q < n_sp)
        def _():
            pl.semaphore_signal(
                barrier, inc=1, device_id={"sp": lax.rem(sp + q, n_sp)},
                device_id_type=pl.DeviceIdType.MESH,
            )
    load_tokens(0).start()
    for i in range(4):
        load_weight(0, i).start()
    load_tokens(1).start()

    lane1 = lax.broadcasted_iota(jnp.int32, (1, LANES), 1)
    first_lanes = lane1 < HEAD_DIM
    half_masks = (
        jnp.where(first_lanes, scale, 0.0).astype(BF16),
        jnp.where(first_lanes, 0.0, scale).astype(BF16),
    )
    lane = lax.broadcasted_iota(jnp.int32, (CHUNK, LANES), 1)
    row = lax.broadcasted_iota(jnp.int32, (CHUNK, LANES), 0)
    same_head = (row < HEAD_DIM) == (lane < HEAD_DIM)
    before = row > lane
    early[...] = jnp.where(before, 1.0, 0.0).astype(BF16)

    pad = cr.shape[1]
    cr[...] = jnp.zeros_like(cr)
    for copy in smalls:
        copy.wait()
    for i in range(4, len(parts)):
        load_weight(0, i).start()
    for p in range(pairs):
        gt[p] = jnp.broadcast_to(
            rgain[p * LANES : (p + 1) * LANES].reshape(1, LANES), (LANES, LANES)
        ).T
    for h in range(heads):
        for c in range(chunks):
            cr[c, h : h + 1, :] = ld[h, :, c * CHUNK : (c + 1) * CHUNK]
    steps = cr[...].reshape(chunks * pad, CHUNK)
    top = steps.astype(BF16)
    rest = steps - top.astype(F32)
    mid = rest.astype(BF16)
    low = (rest - mid.astype(F32)).astype(BF16)
    upto = jnp.where(row <= lane, 1.0, 0.0).astype(BF16)
    sums = jnp.dot(
        jnp.concatenate([top, mid, low], axis=0), upto, preferred_element_type=F32
    )
    n_steps = chunks * pad
    cumulative = sums[:n_steps] + (sums[n_steps : 2 * n_steps] + sums[2 * n_steps :])
    cr[...] = cumulative.reshape(chunks, pad, CHUNK)
    eqr[...] = jnp.exp(cumulative).reshape(chunks, pad, CHUNK)
    ekr[...] = (jnp.exp(cumulative[:, CHUNK - 1 :] - cumulative) * scale).reshape(
        chunks, pad, CHUNK
    )
    filler = jnp.zeros((LANES - n_steps % LANES, CHUNK), F32)
    columns = jnp.concatenate([cumulative, filler], axis=0).T

    def decay(c, h):
        def piece():
            at = c * pad + h
            wide = jnp.broadcast_to(columns[:, at : at + 1], (CHUNK, LANES))
            gap = jnp.where(row <= lane, cr[c, h : h + 1, :] - wide, -jnp.inf)
            dt[c, h // 2, :, (h % 2) * CHUNK : (h % 2 + 1) * CHUNK] = jnp.exp(gap)

        return piece

    def scaled(i):
        def piece():
            span = slice(i * CHUNK, (i + 1) * CHUNK)
            x = xb[0, span, :].astype(F32)
            xb[0, span, :] = (x * gain[tp]).astype(BF16)
            squares = jnp.broadcast_to(
                jnp.sum(x * x, axis=1, keepdims=True), (CHUNK, LANES)
            )
            sq[span, :] = squares

        return piece

    def turn(i):
        def piece():
            sr[0, i : i + 1, :] = sq[i * CHUNK : (i + 1) * CHUNK, :].T[:1]

        return piece

    def invert(i):
        def piece():
            span = slice(i * CHUNK, (i + 1) * CHUNK)
            line = sr[1, i : i + 1, :]
            for phase in range(2, n_tp):
                line = line + sr[phase, i : i + 1, :]
            squares = sq[span, :] + jnp.broadcast_to(line, (LANES, CHUNK)).T
            inv[span, :] = lax.rsqrt(squares / model + EPS)

        return piece

    def project(phase, cols, i=0, parts_of=1):
        def piece():
            size = rows // parts_of
            span = slice(i * size, (i + 1) * size)
            total = jnp.dot(
                xb[phase, span, :], wb[phase, :, cols], preferred_element_type=F32
            )
            if phase > 0:
                total = acc[span, cols] + total
            if phase == n_tp - 1:
                wide = jnp.concatenate([inv[span, :]] * (TILE // LANES), axis=1)
                pb[WINDOW + i * size : WINDOW + (i + 1) * size, cols] = (
                    total * wide
                ).astype(BF16)
            else:
                acc[span, cols] = total

        return piece

    per_half = half // CHUNK
    last = n_tp - 1
    every = [kv_tile] + pair_tiles + query_tiles
    decays = [decay(c, h) for c in range(chunks) for h in range(heads)]
    weave(decays[:heads])
    decays = decays[heads:]
    load_tokens(0).wait()
    weave([scaled(i) for i in range(per_half)])
    pl.semaphore_wait(barrier, n_tp - 1 + sp)
    for q in range(1, n_tp):
        send_tokens(q, 0).start()
    for q in range(1, n_sp):
        @pl.when(sp >= q)
        def _():
            pl.semaphore_signal(
                ready, inc=1, device_id={"sp": lax.rem(sp + n_sp - q, n_sp)},
                device_id_type=pl.DeviceIdType.MESH,
            )
    load_tokens(1).wait()
    wait_weights(0)
    weave(
        [project(0, cols, 0, 2) for cols in every[:2]],
        [scaled(i) for i in range(per_half, chunks)],
    )
    for q in range(1, n_tp):
        send_tokens(q, 1).start()
    cut = len(decays) // len(every)
    weave(
        [project(0, cols, 1, 2) for cols in every[:2]],
        decays[:cut] + [turn(i) for i in range(chunks)],
    )
    for q in range(1, n_tp):
        send_squares(q).start()
    wait_weights(1)
    for phase in range(1, n_tp):
        for i in range(len(parts)):
            load_weight(phase, i).start()
    for q in range(1, n_tp):
        send_exit(q, 1).start()
    for i in range(1, -1, -1):
        load_exit(i).start()
    weave([project(0, cols) for cols in every[2:]], decays[cut:])
    for phase in range(1, n_tp):
        wait_weights(phase + 1)
        send_squares(n_tp - phase).wait_recv()
        all_tokens(n_tp - phase).wait_recv()
        if phase < last:
            weave([project(phase, cols) for cols in every])

    @pl.when(sp + 1 < n_sp)
    def _():
        pl.semaphore_wait(ready, n_sp - 1 - sp)


    def here(c):
        return pl.ds(pl.multiple_of(WINDOW + c * CHUNK, CHUNK), CHUNK)

    def own_state(p):
        def piece(c):
            turned = pb[here(c), c_rv(p)].T
            vt[c, p] = turned
            wide = turned.astype(F32)
            faded = jnp.concatenate(
                [
                    wide[:HEAD_DIM] * ekr[c, 2 * p : 2 * p + 1, :],
                    wide[HEAD_DIM:] * ekr[c, 2 * p + 1 : 2 * p + 2, :],
                ],
                axis=0,
            ).astype(BF16)
            added = jnp.dot(faded, pb[here(c), c_rk(p)], preferred_element_type=F32)
            ub[c, p] = jnp.where(same_head, added, 0.0)

        def pack():
            state = ub[0, p]
            for c in range(1, chunks):
                state = state * fade_row(c, p) + ub[c, p]
            msg[16 + p * HEAD_DIM : 16 + (p + 1) * HEAD_DIM, :] = (
                state[:HEAD_DIM] + state[HEAD_DIM:]
            ).astype(BF16)

        return [functools.partial(piece, c) for c in range(chunks)] + [pack]

    def fade_row(c, p):
        ends = [
            jnp.broadcast_to(eqr[c, h : h + 1, CHUNK - 1 :], (1, LANES))
            for h in (2 * p, 2 * p + 1)
        ]
        return jnp.where(first_lanes, ends[0], ends[1])

    totals = jnp.zeros((16, LANES), F32)
    row16 = lax.broadcasted_iota(jnp.int32, (16, LANES), 0)
    for p in range(pairs):
        total = fade_row(0, p)
        for c in range(1, chunks):
            total = total * fade_row(c, p)
        coarse = total.astype(BF16).astype(F32)
        totals = jnp.where(row16 == 2 * p, coarse, totals)
        totals = jnp.where(row16 == 2 * p + 1, total - coarse, totals)
    msg[:16, :] = totals.astype(BF16)

    def send_states(p):
        for q in range(n_sp - 1, 0, -1):
            @pl.when(sp + q < n_sp)
            def _():
                send_state(q, p).start()

    def double(i):
        def piece():
            span = slice(i * WINDOW, (i + 1) * WINDOW)
            for t in range(kv_w // LANES):
                keys = pb[span, c_ak + t * LANES : c_ak + (t + 1) * LANES]
                swapped = pltpu.roll(keys.astype(F32), HEAD_DIM, 1).astype(BF16)
                values = pb[span, c_av + t * LANES : c_av + (t + 1) * LANES].T
                for e in range(2):
                    g = 2 * t + e
                    kd[g, span, :] = jnp.where(first_lanes == (e == 0), keys, swapped)
                    va[i, g, :HEAD_DIM, :] = values[e * HEAD_DIM : (e + 1) * HEAD_DIM]
                    va[i, g, HEAD_DIM:, :] = jnp.ones((16, WINDOW), BF16)

        return piece

    def halves(cols):
        return [project(last, cols, i, 2) for i in range(2)]

    weave([invert(i) for i in range(chunks)])
    weave(halves(kv_tile) + halves(pair_tiles[0]))
    @pl.when(sp + 1 < n_sp)
    def _():
        send_halo().start()

    weave(own_state(0))
    send_states(0)
    weave(
        [piece for p in range(1, pairs) for piece in halves(pair_tiles[p])],
        [double(i) for i in range(1, blocks + 1)],
    )
    weave(*[own_state(p) for p in range(1, pairs)])
    for p in range(1, pairs):
        send_states(p)
    for q in range(1, n_tp):
        send_exit(q, 0).start()
    weave([piece for cols in query_tiles for piece in halves(cols)])

    per_part = blocks // n_tp

    def block(n):
        part = lax.rem(n // per_part + tp + 1, n_tp)
        return part * per_part + (n + 1) % per_part

    def band(n):
        return pl.ds(pl.multiple_of(block(n) * WINDOW, WINDOW), 2 * WINDOW)

    def score(n):
        def piece(g):
            queries = []
            for h in range(g * group, (g + 1) * group):
                at = c_aq + (h // 2) * LANES
                queries.append(pb[here(block(n)), at : at + LANES] * half_masks[h % 2])
            sc[n, :, g * group * WINDOW : (g + 1) * group * WINDOW] = lax.dot_general(
                kd[g, band(n), :], jnp.concatenate(queries, axis=0), NT,
                preferred_element_type=F32,
            )

        return [functools.partial(piece, g) for g in range(kv_heads)]

    def weigh(n):
        def piece(h):
            cols = slice(h * WINDOW, (h + 1) * WINDOW)
            outside = jnp.where((sp == 0) & (block(n) == 0), -jnp.inf, 0.0).astype(F32)
            s = jnp.where(before, sc[n, :WINDOW, cols] + outside, sc[n, WINDOW:, cols])
            sink_h = jnp.full((1, WINDOW), sink[h], F32)
            top = jnp.maximum(jnp.max(s, axis=0, keepdims=True), sink_h)
            dn[n, h : h + 1, :] = jnp.exp(sink_h - top)
            weights = jnp.exp(s - top).astype(BF16)
            older = weights * early[...]
            pw[n, :WINDOW, cols] = older
            pw[n, WINDOW:, cols] = weights - older

        return [functools.partial(piece, h) for h in range(att_heads)]

    def gather(n):
        def piece(g):
            left = jnp.concatenate([va[block(n), g], va[block(n) + 1, g]], axis=1)
            cols = slice(g * group * WINDOW, (g + 1) * group * WINDOW)
            total = jnp.dot(left, pw[n, :, cols], preferred_element_type=F32)
            for j in range(group):
                h = g * group + j
                cols = slice(j * WINDOW, (j + 1) * WINDOW)
                below = total[HEAD_DIM : HEAD_DIM + 1, cols] + dn[n, h : h + 1, :]
                ao[n, h * HEAD_DIM : (h + 1) * HEAD_DIM, :] = (
                    total[:HEAD_DIM, cols] * (1.0 / below)
                ).astype(BF16)

        def place():
            store = pl.ds(pl.multiple_of(block(n) * WINDOW, WINDOW), WINDOW)
            for p in range(att_pairs):
                hb[store, ret_w + p * LANES : ret_w + (p + 1) * LANES] = ao[
                    n, p * LANES : (p + 1) * LANES, :
                ].T

        return [functools.partial(piece, g) for g in range(kv_heads)] + [place]

    def relate(c):
        def piece(p):
            query = pb[here(c), c_rq + p * LANES : c_rq + (p + 1) * LANES]
            queries = jnp.concatenate([query * half_masks[e] for e in range(2)], axis=0)
            rs[c, p] = lax.dot_general(
                pb[here(c), c_rk(p)], queries, NT, preferred_element_type=F32
            )

        return [functools.partial(piece, p) for p in range(pairs)]

    def fade(c):
        def piece(p):
            rw[c, p] = (rs[c, p] * dt[c, p]).astype(BF16)

        return [functools.partial(piece, p) for p in range(pairs)]

    def recall(c):
        def piece(p):
            total = jnp.dot(vt[c, p], rw[c, p], preferred_element_type=F32)
            ri[c, p, :HEAD_DIM, :] = total[:HEAD_DIM, :CHUNK]
            ri[c, p, HEAD_DIM:, :] = total[HEAD_DIM:, CHUNK:]

        return [functools.partial(piece, p) for p in range(pairs)]

    for i in range(blocks + 2):
        if i % per_part == per_part - 1 and i < blocks:
            @pl.when((tp == n_tp - 1 - i // per_part) & (sp > 0))
            def _():
                send_halo().wait_recv()
                pb[:WINDOW, kv_tile] = halo[...]
                double(0)()

            @pl.when((tp == n_tp - 1 - i // per_part) & (sp == 0))
            def _():
                pb[:WINDOW, kv_tile] = jnp.zeros((WINDOW, 2 * kv_w), BF16)
                double(0)()

        first, second, third = (0 <= i - k < blocks for k in range(3))
        weave(
            (score(i) + relate(i) if first else [])
            + (gather(i - 2) + recall(i - 2) if third else []),
            weigh(i - 1) + fade(i - 1) if second else [],
        )
        for q in range(1, n_tp):
            if i - 1 == q * per_part:
                send_heads(q, 1).start()

    mine = pl.ds(pl.multiple_of(tp * out_rows, out_rows), out_rows)

    def leave(kind, n):
        def piece():
            cols = slice(n * TILE, (n + 1) * TILE)
            inner = slice(kind * ret_w, (kind + 1) * ret_w)
            left = jnp.concatenate(
                [hb[mine, inner]] + [hin[phase - 1, :, inner] for phase in range(1, n_tp)],
                axis=1,
            )
            total = jnp.dot(left, wo[kind, :, cols], preferred_element_type=F32)
            if kind == 1:
                oacc[:, cols] = total
            else:
                out[:, cols] = (oacc[:, cols] + total).astype(BF16)

        return piece

    st[...] = jnp.zeros_like(st)
    for q in range(n_sp - 1, 0, -1):
        @pl.when(sp >= q)
        def _():
            all_states(q).wait_recv()
            tail = inbox[q - 1, :16, :].astype(F32)
            for p in range(pairs):
                part = inbox[q - 1, 16 + p * HEAD_DIM : 16 + (p + 1) * HEAD_DIM, :].astype(F32)
                fade = tail[2 * p : 2 * p + 1] + tail[2 * p + 1 : 2 * p + 2]
                both = jnp.concatenate([part, part], axis=0)
                st[p] = st[p] * fade + jnp.where(same_head, both, 0.0)

    for p in range(pairs):
        state = st[p]
        for c in range(chunks):
            stb[c, p] = state.astype(BF16)
            if c + 1 < chunks:
                state = state * fade_row(c, p) + ub[c, p]

    def finish(c):
        def piece(p):
            query = pb[here(c), c_rq + p * LANES : c_rq + (p + 1) * LANES]
            carried = lax.dot_general(stb[c, p], query, NT, preferred_element_type=F32)
            normed = []
            for e in range(2):
                span = slice(e * HEAD_DIM, (e + 1) * HEAD_DIM)
                h = 2 * p + e
                r = ri[c, p, span, :] + carried[span] * eqr[c, h : h + 1, :]
                square = jnp.sum(r * r, axis=0, keepdims=True)
                normed.append(
                    (r * lax.rsqrt(square * (1.0 / HEAD_DIM) + EPS) * gt[p, span, :]).astype(BF16)
                )
            rows_c = pl.ds(pl.multiple_of(c * CHUNK, CHUNK), CHUNK)
            hb[rows_c, p * LANES : (p + 1) * LANES] = jnp.concatenate(normed, axis=0).T

        return [functools.partial(piece, p) for p in range(pairs)]

    each = chunks // n_tp
    for q in range(1, n_tp):
        first = lax.rem(tp + q, n_tp) * each
        weave([piece for i in range(each) for piece in finish(first + i)])
        send_heads(q, 0).start()
    wait_exit()
    for phase in range(1, n_tp):
        all_exit(n_tp - phase).wait_recv()
        send_heads(n_tp - phase, 1).wait_recv()
    weave(
        [leave(1, n) for n in range(model // TILE)],
        [piece for i in range(each) for piece in finish(tp * each + i)],
    )
    for phase in range(1, n_tp):
        send_heads(n_tp - phase, 0).wait_recv()
    weave([leave(0, n) for n in range(model // TILE)])
    for q in range(1, n_tp):
        send_squares(q).wait_send()
        all_tokens(q).wait_send()
        all_exit(q).wait_send()
        all_heads(q).wait_send()
    for q in range(1, n_sp):
        @pl.when(sp + q < n_sp)
        def _():
            all_states(q).wait_send()

    @pl.when(sp + 1 < n_sp)
    def _():
        send_halo().wait_send()


def shards(n_sp, n_tp, tokens, in_gain, rq, rk, rv, aq, ak, av, log_decay, ret_gain, sink, wr, wa):
    rows, depth = tokens.shape[1:]
    ret_w, att_w, kv_w = rq.shape[1], aq.shape[1], ak.shape[1]
    heads = log_decay.shape[1]
    model = depth * n_tp
    width = 3 * ret_w + att_w + 2 * kv_w
    chunks, pairs, blocks = rows // CHUNK, ret_w // LANES, rows // WINDOW
    att_heads = att_w // HEAD_DIM
    out_rows = rows // n_tp
    later = max(n_sp - 1, 1)
    others = max(n_tp - 1, 1)
    packed = pairs * HEAD_DIM + 16
    pad = 8
    hbm = pl.BlockSpec(memory_space=pltpu.HBM)
    dma = pltpu.SemaphoreType.DMA
    result = pl.pallas_call(
        functools.partial(layer, n_sp, n_tp),
        out_shape=pltpu.VMEM((out_rows, model), BF16),
        in_specs=[hbm] * 13,
        out_specs=pl.BlockSpec(memory_space=pltpu.VMEM),
        scratch_shapes=[
            pltpu.VMEM((n_tp, rows, depth), BF16),
            pltpu.VMEM((n_tp, depth, width), BF16),
            pltpu.VMEM((rows, width), F32),
            pltpu.VMEM((WINDOW + rows, width), BF16),
            pltpu.VMEM((rows, LANES), F32),
            pltpu.VMEM((rows, LANES), F32),
            pltpu.VMEM((chunks, pad, CHUNK), F32),
            pltpu.VMEM((chunks, pad, CHUNK), F32),
            pltpu.VMEM((chunks, pad, CHUNK), F32),
            pltpu.VMEM((chunks, pairs, CHUNK, 2 * CHUNK), F32),
            pltpu.VMEM((chunks, pairs, LANES, CHUNK), BF16),
            pltpu.VMEM((chunks, pairs, LANES, LANES), F32),
            pltpu.VMEM((pairs, LANES, LANES), F32),
            pltpu.VMEM((chunks, pairs, LANES, LANES), BF16),
            pltpu.VMEM((chunks, pairs, LANES, CHUNK), F32),
            pltpu.VMEM((WINDOW, WINDOW), BF16),
            pltpu.VMEM((kv_w // HEAD_DIM, WINDOW + rows, LANES), BF16),
            pltpu.VMEM((blocks + 1, kv_w // HEAD_DIM, HEAD_DIM + 16, WINDOW), BF16),
            pltpu.VMEM((blocks, 2 * WINDOW, att_heads * WINDOW), F32),
            pltpu.VMEM((blocks, 2 * WINDOW, att_heads * WINDOW), BF16),
            pltpu.VMEM((blocks, 8, WINDOW), F32),
            pltpu.VMEM((blocks, att_w, WINDOW), BF16),
            pltpu.VMEM((chunks, pairs, CHUNK, 2 * CHUNK), F32),
            pltpu.VMEM((chunks, pairs, CHUNK, 2 * CHUNK), BF16),
            pltpu.VMEM((packed, LANES), BF16),
            pltpu.VMEM((later, packed, LANES), BF16),
            pltpu.VMEM((WINDOW, 2 * kv_w), BF16),
            pltpu.VMEM((n_tp, 8, CHUNK), F32),
            pltpu.VMEM((rows, ret_w + att_w), BF16),
            pltpu.VMEM((others, out_rows, ret_w + att_w), BF16),
            pltpu.VMEM((2, n_tp * ret_w, model), BF16),
            pltpu.VMEM((out_rows, model), F32),
            pltpu.VMEM((pairs, LANES, LANES), F32),
            pltpu.VMEM((n_tp, 1, depth), F32),
            pltpu.VMEM((heads, 1, rows), F32),
            pltpu.VMEM((ret_w,), F32),
            pltpu.SMEM(sink.shape, F32),
            dma((4,)), dma((2,)), dma((n_tp + 1,)), dma,
            dma((others,)), dma((others,)),
            dma((others,)), dma((others,)),
            dma((others,)), dma((others, 2)),
            dma((later,)), dma((later,)),
            dma((others,)), dma((others,)),
            dma, dma, pltpu.SemaphoreType.REGULAR,
        ],
        compiler_params=pltpu.CompilerParams(
            collective_id=0, has_side_effects=True, vmem_limit_bytes=62 * 1024 * 1024
        ),
    )(
        tokens[0], in_gain.reshape(n_tp, 1, depth), rq, rk, rv, aq, ak, av,
        jnp.transpose(log_decay, (1, 0, 2)), ret_gain, sink, wr, wa,
    )
    return result[None]


def solution(mesh):
    n_sp, n_tp = mesh.shape["sp"], mesh.shape["tp"]
    return jax.shard_map(
        functools.partial(shards, n_sp, n_tp),
        mesh=mesh,
        in_specs=(
            P("fs", "sp", "tp"),
            P(),
            P(None, "tp"),
            P(None, "tp"),
            P(None, "tp"),
            P(None, "tp"),
            P(None, "tp"),
            P(None, "tp"),
            P("fs", "tp", "sp"),
            P("tp"),
            P("tp"),
            P("tp", None),
            P("tp", None),
        ),
        out_specs=P("fs", ("sp", "tp"), None),
        check_vma=False,
    )
```

time: 24.4 us -> 19.5 us (0.80)
  Pallas kernels: 23.1 us -> 18.2 us
    pallas_call x1, Pallas kernels: 23.1 us -> 18.2 us  [shards(): pl.pallas_call(functools.partial(layer, n_sp, n_tp), out_shape=pltpu.VMEM...]
where the time goes in v2:
time: 19.5 us; the launch traced here: 19.4 us
  Pallas kernels  18.2 us (93%)
  local copies, waits for them, and re-layouts  1.15 us (6%)
    pallas_call x1, Pallas kernels, shards(): pl.pallas_call(functools.partial(layer, n_sp, n_tp), out_shape=pltpu.VMEM...  18.2 us
    unnamed x1, local copies, waits for them, and re-layouts  1.15 us

profile of v2, /device:TPU:19, one launch (start us, length us, event | category | flops | bytes accessed | tf_op | source)
XLA Modules:
  0.0 19.4 jit_solution(2442589206221153920)
XLA Ops:
  0.0 18.2 %shard_map.127 = bf16[384,2048]{1,0:T(8,128)(2,1)S(1)} custom-call(bf16[768,1024]{1,0:T(8,128)(2,1)} %bitcast.5, f32[2,1,1024]{2,1,0:T(1,128)} %bitcast.7, bf16[2048,384]{1,0:T(8,128)(2,1)} %rq.1, bf16[2048,384]{1,0:T(8,128)(2,1)} %rk.1, bf16[2048,384]{1,0:T(8,128)(2,1)} %rv.1, bf16[2048,384]{1,0:T(8,128)(2,1)} %aq.1, bf16[2048,128]{1,0:T(8,128)(2,1)} %ak.1, ...), custom_call_target="tpu_custom_call" | custom-call | tf_op jit(solution)/shard_map/pallas_call | solution.py:669
  18.2 1.1 %copy.15 = bf16[1,384,2048]{2,1,0:T(8,128)(2,1)} copy(bf16[1,384,2048]{2,1,0:T(8,128)(2,1)S(1)} %bitcast.4) | data formatting | bytes 3145728

commit v3 on v2

--- a/solution.py
+++ b/solution.py
@@ -118,7 +118,7 @@
         here_ = wo.at[:, pl.ds((n_tp - q) * ret_w, ret_w), :]
         return pltpu.make_async_remote_copy(
             src_ref=here_, dst_ref=here_,
-            send_sem=wo_send.at[q - 1], recv_sem=wo_recv.at[n_tp - q - 1],
+            send_sem=wo_send.at[q - 1], recv_sem=wo_recv.at[n_tp - q - 1, 0],
             device_id={"tp": lax.rem(tp + q, n_tp)}, device_id_type=pl.DeviceIdType.MESH,
         )
 
@@ -156,9 +156,9 @@
     def send_exit(q, i):
         ref = (wr, wa)[i]
         return pltpu.make_async_remote_copy(
-            src_ref=ref,
+            src_ref=wo.at[i, pl.ds(0, ref.shape[0]), :],
             dst_ref=wo.at[i, pl.ds((n_tp - q) * ref.shape[0], ref.shape[0]), :],
-            send_sem=wo_send.at[q - 1], recv_sem=wo_recv.at[n_tp - q - 1],
+            send_sem=wo_send.at[q - 1], recv_sem=wo_recv.at[n_tp - q - 1, i],
             device_id={"tp": lax.rem(tp + q, n_tp)}, device_id_type=pl.DeviceIdType.MESH,
         )
 
@@ -353,22 +353,15 @@
     for phase in range(1, n_tp):
         for i in range(len(parts)):
             load_weight(phase, i).start()
-    for q in range(1, n_tp):
-        send_exit(q, 1).start()
     for i in range(1, -1, -1):
         load_exit(i).start()
-    weave([project(0, cols) for cols in every[2:]], decays[cut:])
+    weave([project(0, cols, i, 2) for cols in every[2:] for i in range(2)], decays[cut:])
     for phase in range(1, n_tp):
         wait_weights(phase + 1)
         send_squares(n_tp - phase).wait_recv()
         all_tokens(n_tp - phase).wait_recv()
         if phase < last:
             weave([project(phase, cols) for cols in every])
-
-    @pl.when(sp + 1 < n_sp)
-    def _():
-        pl.semaphore_wait(ready, n_sp - 1 - sp)
-
 
     def here(c):
         return pl.ds(pl.multiple_of(WINDOW + c * CHUNK, CHUNK), CHUNK)
@@ -444,6 +437,7 @@
     weave(halves(kv_tile) + halves(pair_tiles[0]))
     @pl.when(sp + 1 < n_sp)
     def _():
+        pl.semaphore_wait(ready, n_sp - 1 - sp)
         send_halo().start()
 
     weave(own_state(0))
@@ -455,8 +449,9 @@
     weave(*[own_state(p) for p in range(1, pairs)])
     for p in range(1, pairs):
         send_states(p)
+    wait_exit()
     for q in range(1, n_tp):
-        send_exit(q, 0).start()
+        send_exit(q, 1).start()
     weave([piece for cols in query_tiles for piece in halves(cols)])
 
     per_part = blocks // n_tp
@@ -564,6 +559,7 @@
         for q in range(1, n_tp):
             if i - 1 == q * per_part:
                 send_heads(q, 1).start()
+                send_exit(q, 0).start()
 
     mine = pl.ds(pl.multiple_of(tp * out_rows, out_rows), out_rows)
 
@@ -583,6 +579,12 @@
 
         return piece
 
+    for phase in range(1, n_tp):
+        send_exit(n_tp - phase, 1).wait_recv()
+        send_heads(n_tp - phase, 1).wait_recv()
+    exits = [leave(1, n) for n in range(model // TILE)]
+    share = len(exits) // 2
+    weave(exits[:share])
     st[...] = jnp.zeros_like(st)
     for q in range(n_sp - 1, 0, -1):
         @pl.when(sp >= q)
@@ -625,15 +627,12 @@
         first = lax.rem(tp + q, n_tp) * each
         weave([piece for i in range(each) for piece in finish(first + i)])
         send_heads(q, 0).start()
-    wait_exit()
-    for phase in range(1, n_tp):
-        all_exit(n_tp - phase).wait_recv()
-        send_heads(n_tp - phase, 1).wait_recv()
     weave(
         [leave(1, n) for n in range(model // TILE)],
         [piece for i in range(each) for piece in finish(tp * each + i)],
     )
     for phase in range(1, n_tp):
+        send_exit(n_tp - phase, 0).wait_recv()
         send_heads(n_tp - phase, 0).wait_recv()
     weave([leave(0, n) for n in range(model // TILE)])
     for q in range(1, n_tp):
@@ -711,7 +710,7 @@
             pltpu.SMEM(sink.shape, F32),
             dma((4,)), dma((2,)), dma((n_tp + 1,)), dma,
             dma((others,)), dma((others,)),
-            dma((others,)), dma((others,)),
+            dma((others,)), dma((others, 2)),
             dma((others,)), dma((others, 2)),
             dma((later,)), dma((later,)),
             dma((others,)), dma((others,)),

time: 19.5 us -> 18.8 us (0.964)
  Pallas kernels: 18.2 us -> 17.5 us
    pallas_call x1, Pallas kernels: 18.2 us -> 17.5 us  [shards(): pl.pallas_call(functools.partial(layer, n_sp, n_tp), out_shape=pltpu.VMEM...]
where the time goes in v3:
time: 18.8 us; the launch traced here: 18.6 us
  Pallas kernels  17.5 us (93%)
  local copies, waits for them, and re-layouts  1.15 us (6%)
    pallas_call x1, Pallas kernels, shards(): pl.pallas_call(functools.partial(layer, n_sp, n_tp), out_shape=pltpu.VMEM...  17.5 us
    unnamed x1, local copies, waits for them, and re-layouts  1.15 us

profile of v3, /device:TPU:19, one launch (start us, length us, event | category | flops | bytes accessed | tf_op | source)
XLA Modules:
  0.0 18.6 jit_solution(16714678145527618434)
XLA Ops:
  0.0 17.5 %shard_map.127 = bf16[384,2048]{1,0:T(8,128)(2,1)S(1)} custom-call(bf16[768,1024]{1,0:T(8,128)(2,1)} %bitcast.5, f32[2,1,1024]{2,1,0:T(1,128)} %bitcast.7, bf16[2048,384]{1,0:T(8,128)(2,1)} %rq.1, bf16[2048,384]{1,0:T(8,128)(2,1)} %rk.1, bf16[2048,384]{1,0:T(8,128)(2,1)} %rv.1, bf16[2048,384]{1,0:T(8,128)(2,1)} %aq.1, bf16[2048,128]{1,0:T(8,128)(2,1)} %ak.1, ...), custom_call_target="tpu_custom_call" | custom-call | tf_op jit(solution)/shard_map/pallas_call | solution.py:668
  17.5 1.1 %copy.15 = bf16[1,384,2048]{2,1,0:T(8,128)(2,1)} copy(bf16[1,384,2048]{2,1,0:T(8,128)(2,1)S(1)} %bitcast.4) | data formatting | bytes 3145728

commit v4 on v3

--- a/solution.py
+++ b/solution.py
@@ -12,6 +12,7 @@
 CHUNK = 128
 LANES = 128
 TILE = 256
+PARTS = 4
 EPS = 1e-06
 F32 = jnp.float32
 BF16 = jnp.bfloat16
@@ -34,9 +35,9 @@
     tok, gain_in, rq, rk, rv, aq, ak, av, ld_in, rgain_in, sink_in, wr, wa,
     out,
     xb, wb, acc, pb, sq, inv, cr, eqr, ekr, dt, vt, ub, st, stb, ri, early, kd, va, sc, pw, dn, ao,
-    rs, rw, msg, inbox, halo, sr, hb, hin, wo, oacc, gt,
+    rs, rw, msg, inbox, tot, tin, halo, sr, hb, hin, wo, oacc, gt,
     gain, ld, rgain, sink, small_sem, tok_sem, w_sem, wo_sem, x_send, x_recv, wo_send, wo_recv,
-    h_send, h_recv, m_send, m_recv, s_send, s_recv, halo_send, halo_recv, ready,
+    h_send, h_recv, m_send, m_recv, t_send, t_recv, s_send, s_recv, halo_send, halo_recv, ready,
 ):
     tp = lax.axis_index("tp")
     sp = lax.axis_index("sp")
@@ -131,6 +132,13 @@
             device_id={"tp": target}, device_id_type=pl.DeviceIdType.MESH,
         )
 
+    def send_total(q):
+        return pltpu.make_async_remote_copy(
+            src_ref=tot, dst_ref=tin.at[q - 1],
+            send_sem=t_send.at[q - 1], recv_sem=t_recv.at[q - 1],
+            device_id={"sp": lax.rem(sp + q, n_sp)}, device_id_type=pl.DeviceIdType.MESH,
+        )
+
     def all_states(q):
         return pltpu.make_async_remote_copy(
             src_ref=msg, dst_ref=inbox.at[q - 1],
@@ -153,11 +161,21 @@
             device_id={"tp": lax.rem(tp + q, n_tp)}, device_id_type=pl.DeviceIdType.MESH,
         )
 
-    def send_exit(q, i):
-        ref = (wr, wa)[i]
-        return pltpu.make_async_remote_copy(
-            src_ref=wo.at[i, pl.ds(0, ref.shape[0]), :],
-            dst_ref=wo.at[i, pl.ds((n_tp - q) * ref.shape[0], ref.shape[0]), :],
+    def send_exit(q, i, part):
+        size = ret_w // PARTS
+        span = pl.ds(part * size, size)
+        source = (wr, wa)[i].at[span, :] if i == 1 and part < PARTS // 2 else wo.at[i, span, :]
+        return pltpu.make_async_remote_copy(
+            src_ref=source,
+            dst_ref=wo.at[i, pl.ds((n_tp - q) * ret_w + part * size, size), :],
+            send_sem=wo_send.at[q - 1], recv_sem=wo_recv.at[n_tp - q - 1, i],
+            device_id={"tp": lax.rem(tp + q, n_tp)}, device_id_type=pl.DeviceIdType.MESH,
+        )
+
+    def whole_exit(q, i):
+        place = wo.at[i, pl.ds((n_tp - q) * ret_w, ret_w), :]
+        return pltpu.make_async_remote_copy(
+            src_ref=place, dst_ref=place,
             send_sem=wo_send.at[q - 1], recv_sem=wo_recv.at[n_tp - q - 1, i],
             device_id={"tp": lax.rem(tp + q, n_tp)}, device_id_type=pl.DeviceIdType.MESH,
         )
@@ -173,7 +191,7 @@
         )
 
     def send_state(q, p):
-        span = pl.ds(0, 16 + HEAD_DIM) if p == 0 else pl.ds(16 + p * HEAD_DIM, HEAD_DIM)
+        span = pl.ds(p * HEAD_DIM, HEAD_DIM)
         return pltpu.make_async_remote_copy(
             src_ref=msg.at[span, :], dst_ref=inbox.at[q - 1, span, :],
             send_sem=m_send.at[q - 1], recv_sem=m_recv.at[q - 1],
@@ -385,7 +403,7 @@
             state = ub[0, p]
             for c in range(1, chunks):
                 state = state * fade_row(c, p) + ub[c, p]
-            msg[16 + p * HEAD_DIM : 16 + (p + 1) * HEAD_DIM, :] = (
+            msg[p * HEAD_DIM : (p + 1) * HEAD_DIM, :] = (
                 state[:HEAD_DIM] + state[HEAD_DIM:]
             ).astype(BF16)
 
@@ -398,21 +416,20 @@
         ]
         return jnp.where(first_lanes, ends[0], ends[1])
 
-    totals = jnp.zeros((16, LANES), F32)
-    row16 = lax.broadcasted_iota(jnp.int32, (16, LANES), 0)
-    for p in range(pairs):
-        total = fade_row(0, p)
+    totals = jnp.zeros((1, LANES), F32)
+    for h in range(heads):
+        total = eqr[0, h : h + 1, CHUNK - 1 :]
         for c in range(1, chunks):
-            total = total * fade_row(c, p)
-        coarse = total.astype(BF16).astype(F32)
-        totals = jnp.where(row16 == 2 * p, coarse, totals)
-        totals = jnp.where(row16 == 2 * p + 1, total - coarse, totals)
-    msg[:16, :] = totals.astype(BF16)
+            total = total * eqr[c, h : h + 1, CHUNK - 1 :]
+        totals = jnp.where(lane1 == h, jnp.broadcast_to(total, (1, LANES)), totals)
+    tot[...] = totals
 
     def send_states(p):
         for q in range(n_sp - 1, 0, -1):
             @pl.when(sp + q < n_sp)
             def _():
+                if p == 0:
+                    send_total(q).start()
                 send_state(q, p).start()
 
     def double(i):
@@ -433,15 +450,25 @@
     def halves(cols):
         return [project(last, cols, i, 2) for i in range(2)]
 
+    for q in range(1, n_tp):
+        send_exit(q, 1, 0).start()
     weave([invert(i) for i in range(chunks)])
     weave(halves(kv_tile) + halves(pair_tiles[0]))
-    @pl.when(sp + 1 < n_sp)
+    @pl.when((sp > 0) & (sp + 1 < n_sp))
     def _():
         pl.semaphore_wait(ready, n_sp - 1 - sp)
         send_halo().start()
 
     weave(own_state(0))
+
+    @pl.when((sp == 0) & (sp + 1 < n_sp))
+    def _():
+        pl.semaphore_wait(ready, n_sp - 1 - sp)
+        send_halo().start()
+
     send_states(0)
+    for q in range(1, n_tp):
+        send_exit(q, 1, 1).start()
     weave(
         [piece for p in range(1, pairs) for piece in halves(pair_tiles[p])],
         [double(i) for i in range(1, blocks + 1)],
@@ -451,7 +478,9 @@
         send_states(p)
     wait_exit()
     for q in range(1, n_tp):
-        send_exit(q, 1).start()
+        for part in range(2, PARTS):
+            send_exit(q, 1, part).start()
+        send_exit(q, 0, 0).start()
     weave([piece for cols in query_tiles for piece in halves(cols)])
 
     per_part = blocks // n_tp
@@ -559,7 +588,8 @@
         for q in range(1, n_tp):
             if i - 1 == q * per_part:
                 send_heads(q, 1).start()
-                send_exit(q, 0).start()
+                for part in range(1, PARTS):
+                    send_exit(q, 0, part).start()
 
     mine = pl.ds(pl.multiple_of(tp * out_rows, out_rows), out_rows)
 
@@ -580,7 +610,7 @@
         return piece
 
     for phase in range(1, n_tp):
-        send_exit(n_tp - phase, 1).wait_recv()
+        whole_exit(n_tp - phase, 1).wait_recv()
         send_heads(n_tp - phase, 1).wait_recv()
     exits = [leave(1, n) for n in range(model // TILE)]
     share = len(exits) // 2
@@ -590,10 +620,15 @@
         @pl.when(sp >= q)
         def _():
             all_states(q).wait_recv()
-            tail = inbox[q - 1, :16, :].astype(F32)
+            send_total(q).wait_recv()
+            tail = tin[q - 1]
             for p in range(pairs):
-                part = inbox[q - 1, 16 + p * HEAD_DIM : 16 + (p + 1) * HEAD_DIM, :].astype(F32)
-                fade = tail[2 * p : 2 * p + 1] + tail[2 * p + 1 : 2 * p + 2]
+                part = inbox[q - 1, p * HEAD_DIM : (p + 1) * HEAD_DIM, :].astype(F32)
+                fade = jnp.where(
+                    first_lanes,
+                    jnp.broadcast_to(tail[:, 2 * p : 2 * p + 1], (1, LANES)),
+                    jnp.broadcast_to(tail[:, 2 * p + 1 : 2 * p + 2], (1, LANES)),
+                )
                 both = jnp.concatenate([part, part], axis=0)
                 st[p] = st[p] * fade + jnp.where(same_head, both, 0.0)
 
@@ -632,7 +667,7 @@
         [piece for i in range(each) for piece in finish(tp * each + i)],
     )
     for phase in range(1, n_tp):
-        send_exit(n_tp - phase, 0).wait_recv()
+        whole_exit(n_tp - phase, 0).wait_recv()
         send_heads(n_tp - phase, 0).wait_recv()
     weave([leave(0, n) for n in range(model // TILE)])
     for q in range(1, n_tp):
@@ -644,6 +679,7 @@
         @pl.when(sp + q < n_sp)
         def _():
             all_states(q).wait_send()
+            send_total(q).wait_send()
 
     @pl.when(sp + 1 < n_sp)
     def _():
@@ -661,7 +697,7 @@
     out_rows = rows // n_tp
     later = max(n_sp - 1, 1)
     others = max(n_tp - 1, 1)
-    packed = pairs * HEAD_DIM + 16
+    packed = pairs * HEAD_DIM
     pad = 8
     hbm = pl.BlockSpec(memory_space=pltpu.HBM)
     dma = pltpu.SemaphoreType.DMA
@@ -697,6 +733,8 @@
             pltpu.VMEM((chunks, pairs, CHUNK, 2 * CHUNK), BF16),
             pltpu.VMEM((packed, LANES), BF16),
             pltpu.VMEM((later, packed, LANES), BF16),
+            pltpu.VMEM((1, LANES), F32),
+            pltpu.VMEM((later, 1, LANES), F32),
             pltpu.VMEM((WINDOW, 2 * kv_w), BF16),
             pltpu.VMEM((n_tp, 8, CHUNK), F32),
             pltpu.VMEM((rows, ret_w + att_w), BF16),
@@ -712,6 +750,7 @@
             dma((others,)), dma((others,)),
             dma((others,)), dma((others, 2)),
             dma((others,)), dma((others, 2)),
+            dma((later,)), dma((later,)),
             dma((later,)), dma((later,)),
             dma((others,)), dma((others,)),
             dma, dma, pltpu.SemaphoreType.REGULAR,

time: 18.8 us -> 19 us (1.011)
  no operation moved by 1% of the time
where the time goes in v4:
time: 19 us; the launch traced here: 18.8 us
  Pallas kernels  17.6 us (93%)
  local copies, waits for them, and re-layouts  1.15 us (6%)
    pallas_call x1, Pallas kernels, shards(): pl.pallas_call(functools.partial(layer, n_sp, n_tp), out_shape=pltpu.VMEM...  17.6 us
    unnamed x1, local copies, waits for them, and re-layouts  1.15 us

profile of v4, /device:TPU:19, one launch (start us, length us, event | category | flops | bytes accessed | tf_op | source)
XLA Modules:
  0.0 18.8 jit_solution(11286233227352771599)
XLA Ops:
  0.0 17.6 %shard_map.127 = bf16[384,2048]{1,0:T(8,128)(2,1)S(1)} custom-call(bf16[768,1024]{1,0:T(8,128)(2,1)} %bitcast.5, f32[2,1,1024]{2,1,0:T(1,128)} %bitcast.7, bf16[2048,384]{1,0:T(8,128)(2,1)} %rq.1, bf16[2048,384]{1,0:T(8,128)(2,1)} %rk.1, bf16[2048,384]{1,0:T(8,128)(2,1)} %rv.1, bf16[2048,384]{1,0:T(8,128)(2,1)} %aq.1, bf16[2048,128]{1,0:T(8,128)(2,1)} %ak.1, ...), custom_call_target="tpu_custom_call" | custom-call | tf_op jit(solution)/shard_map/pallas_call | solution.py:704
  17.6 1.1 %copy.15 = bf16[1,384,2048]{2,1,0:T(8,128)(2,1)} copy(bf16[1,384,2048]{2,1,0:T(8,128)(2,1)S(1)} %bitcast.4) | data formatting | bytes 3145728
